TPU v7x, 512 devices: a whole 4x8x8 slice. The times are simulated.
512 devices in a mesh: kv: 64 (over z, y), tp: 8 (over x, core).
Axes of the slice: x: 4, y: 8, z: 8, core: 2. Of those that a mesh axis runs over, the one named last changes fastest.
Arguments:
- queries: bfloat16 [8192, 1024], P('kv', 'tp'), may hold values from -4 to 4
- keys: bfloat16 [8192, 1024], P('kv', 'tp'), may hold values from -4 to 4
- values: bfloat16 [8192, 1024], P('kv', 'tp'), may hold values from -4 to 4
- cotangent: bfloat16 [8192, 1024], P('kv', 'tp'), may hold values from -4 to 4
- log_sum: float32 [16, 8192], P('tp', 'kv'), may hold values from 4.5 to 7.5
- chosen: int32 [16, 256, 12], P('tp'), may hold values from 0 to 255, as said below
- normed_input: bfloat16 [8192, 2048], P('kv', 'tp'), may hold values from -0.0625 to 0.0625
Outputs:
- grad_queries: bfloat16 [8192, 1024], P('kv', 'tp')
- grad_keys: bfloat16 [8192, 1024], P('kv', 'tp')
- grad_values: bfloat16 [8192, 1024], P('kv', 'tp')
- grad_weight: float32 [2048, 1024], P('kv', 'tp')
Inputs may be any that keep to these rules, and one draw needn't show every extreme that they name: `chosen`: for each head, the distinct blocks below their own query block that the query blocks of one device's 128 positions choose include at most 1 block of any one device's span of 128 positions, and exactly 1 for some pairs of devices. Within one list the entries below the query block's own index are distinct.
All inputs are finite; a program needn't handle non-finite values.
Results may differ from a plain program's by a relative error of at most 0.0085.
Values may be sent and summed in bfloat16 or wider, within the bound.
A program may use at most 64 MiB of HBM per device.

v0:
```python
import functools

import jax
import jax.numpy as jnp
from jax import lax
from jax.experimental import pallas as pl
from jax.experimental.pallas import tpu as pltpu
from jax.sharding import PartitionSpec as P

HD = 64
BLK = 32
MASKED = -1e30
MESH = pl.DeviceIdType.MESH
F32 = jnp.float32
BF16 = jnp.bfloat16


def dot(a, b, ca, cb):
    return lax.dot_general(a, b, (((ca,), (cb,)), ((), ())), preferred_element_type=F32)


def kernel(
    n, tp, g, q_in, k_in, v_in, c_in, lse_in, pick_in, x_in,
    gq_ref, gk_ref, gv_ref, gw_ref,
    q_ref, k_ref, v_ref, c_ref, lse_ref, pick_ref, x_ref, insem, bias, hot, kvs, kvt, dkvs, dkvr, gko, gvo, xs, xr, dqr, gs, gr,
    ssem, rsem, xssem, xrsem, dssem, drsem, gssem, grsem,
):
    r = n // g
    tok, cols = q_ref.shape
    sel, heads, blocks = pick_ref.shape
    bd = tok // BLK
    wide = 2 * HD
    pairs = cols // wide
    scale = HD ** (-0.5)
    rt = r // tp
    w = x_ref.shape[1] // (rt * g)
    me, t = lax.axis_index("kv"), lax.axis_index("tp")
    z, j = me // g, lax.rem(me, g)
    rows = n * BLK

    loads = {}
    for i, (a, b) in enumerate((
        (pick_in, pick_ref), (k_in, k_ref), (v_in, v_ref), (x_in, x_ref),
        (q_in, q_ref), (c_in, c_ref), (lse_in, lse_ref),
    )):
        loads[i] = pltpu.make_async_copy(a, b, insem.at[i])
        loads[i].start()

    def iota(shape, dim):
        return lax.broadcasted_iota(jnp.int32, shape, dim)

    def each(low, high, fn):
        def step(i, carry):
            fn(i)
            return carry
        lax.fori_loop(low, high, step, 0)

    def kv_copy(h, there, slot):
        return pltpu.make_async_remote_copy(
            src_ref=kvs.at[h, there], dst_ref=kvt.at[h, slot], send_sem=ssem.at[0, h, there],
            recv_sem=rsem.at[0, h, slot], device_id=(there, t), device_id_type=MESH)

    def back_copy(h, there, slot):
        return pltpu.make_async_remote_copy(
            src_ref=dkvs.at[h, there], dst_ref=dkvr.at[h, slot], send_sem=ssem.at[1, h, there],
            recv_sem=rsem.at[1, h, slot], device_id=(there, t), device_id_type=MESH)

    def x_copy(p, t2, at, t3):
        return pltpu.make_async_remote_copy(
            src_ref=xs.at[p], dst_ref=xr.at[at, pl.ds(t3 * rt, rt)],
            send_sem=xssem.at[p, t2], recv_sem=xrsem.at[at, t3],
            device_id=(z * g + p, t2), device_id_type=MESH)

    def dq_copy(h, p, slot):
        return pltpu.make_async_remote_copy(
            src_ref=dqr.at[h, j], dst_ref=dqr.at[h, slot], send_sem=dssem.at[h, p], recv_sem=drsem.at[h, slot],
            device_id=(z * g + p, t), device_id_type=MESH)

    def gw_copy(h, zz, slot):
        return pltpu.make_async_remote_copy(
            src_ref=gs.at[h, zz], dst_ref=gr.at[h, slot], send_sem=gssem.at[h, zz], recv_sem=grsem.at[h, slot],
            device_id=(zz * g + j, t), device_id_type=MESH)

    def each_x(fn):
        def step(i):
            p, t2 = lax.rem(j + i // tp, g), lax.rem(i, tp)

            @pl.when((p != j) | (t2 != t))
            def _():
                fn(p, t2)
        each(0, g * tp, step)

    pool = (iota((blocks, n), 0) // bd == iota((blocks, n), 1)).astype(BF16)
    spread = (iota((heads, cols), 1) // HD == iota((heads, cols), 0)).astype(BF16)
    later = iota((n, cols), 0) > me
    loads[0].wait()
    for b in range(bd):
        hit = jnp.zeros((heads, blocks), jnp.bool_)
        for s in range(sel):
            hit = hit | (pick_ref[s] == me * bd + b)
        count = dot(jnp.where(hit, 1.0, 0.0).astype(BF16), pool, 1, 0)
        taken = dot(count.astype(BF16), spread, 0, 0)
        hot[:, b, :] = jnp.where((taken > 0.5) & later, 1.0, 0.0)

    def picked(ref, d, c):
        out = None
        for b in range(bd):
            one = jnp.broadcast_to(hot[d, b : b + 1, c : c + wide], (BLK, wide)).astype(BF16)
            term = ref[b * BLK : (b + 1) * BLK, c : c + wide] * one
            out = term if out is None else out + term
        return out

    def send_kv(h):
        def step(i):
            d = (r - 1 - i // g) * g + lax.rem(j + lax.rem(i, g), g)

            @pl.when(d > me)
            def _():
                kvs[h, d, 0] = picked(k_ref, d, h * wide)
                kvs[h, d, 1] = picked(v_ref, d, h * wide)
                kv_copy(h, d, me).start()
        each(0, (r - z) * g, step)

    def send_back(h):
        def step(i):
            o = (i // g) * g + lax.rem(j + lax.rem(i, g), g)

            @pl.when(o < me)
            def _():
                back_copy(h, o, me).start()
        each(0, (z + 1) * g, step)

    loads[1].wait()
    loads[2].wait()
    for h in range(pairs):
        send_kv(h)

    loads[3].wait()
    for p in range(g):
        for zl in range(rt):
            at = (zl * g + p) * w
            xs[p, zl] = x_ref[:, at : at + w]
    each_x(lambda p, t2: x_copy(p, t2, j, t).start())
    xr[j, pl.ds(t * rt, rt)] = xs[j]

    def clear(o):
        for h in range(pairs):
            kvt[h, o] = jnp.zeros(kvt.shape[2:], BF16)
    each(me, n, clear)

    at_block = me * bd + iota((blocks, tok), 1) // BLK
    mine = (iota((blocks, tok), 0) == at_block).astype(F32)
    ids = pick_ref[...].astype(F32).reshape(sel * heads, blocks)
    ids = dot(ids.astype(BF16), mine.astype(BF16), 1, 0)
    ids = (ids + 0.5).astype(jnp.int32).reshape(sel, heads, tok)
    ids = jnp.where(ids < me * bd + iota(ids.shape, 2) // BLK, ids, n * bd)
    owner = ids // bd
    for i in (4, 5, 6):
        loads[i].wait()
    less = -lse_ref[...]

    def put(row, need):
        line = less if need is None else jnp.where(need, less, MASKED)
        for h in range(heads):
            bias[h // 2, row, :, (h % 2) * tok : (h % 2 + 1) * tok] = line[h : h + 1, :]

    for o in range(n):
        need = jnp.zeros((heads, tok), jnp.bool_)
        for s in range(sel):
            need = need | (owner[s] == o)
        put(o, need & (jnp.zeros((heads, tok), jnp.int32) + o < me))
    for b in range(bd):
        need = jnp.zeros((heads, tok), jnp.bool_)
        for s in range(sel):
            need = need | (ids[s] == me * bd + b)
        put(n + b, need)
    put(n + bd, None)

    low = iota((tok, wide), 1) < HD
    key_at = iota((tok, 2 * tok), 0)
    query_at = lax.rem(iota((tok, 2 * tok), 1), tok)
    causal = (key_at // BLK == query_at // BLK) & (key_at <= query_at)

    def stacked(ref, c):
        part = ref[:, c : c + wide]
        zero = jnp.zeros_like(part)
        return jnp.concatenate([jnp.where(low, part, zero), jnp.where(low, zero, part)], axis=0)

    def attend(h):
        c = h * wide
        qs, cs = stacked(q_ref, c), stacked(c_ref, c)
        ko, vo = k_ref[:, c : c + wide], v_ref[:, c : c + wide]
        ob = jnp.broadcast_to(bias[h, n : n + bd], (bd, BLK, 2 * tok)).reshape(tok, 2 * tok)
        ob = jnp.where(causal, bias[h, n + bd], ob)
        own = jnp.exp(dot(ko, qs, 1, 1) * scale + ob)
        vdo = dot(vo, cs, 1, 1)
        gvo[:, c : c + wide] = dot(own.astype(BF16), cs, 1, 0)
        each(0, me, lambda o: kv_copy(h, o, o).wait_recv())
        kp = kvt[h, :, 0].reshape(rows, wide)
        vp = kvt[h, :, 1].reshape(rows, wide)
        st = (dot(kp, qs, 1, 1) * scale).reshape(n, BLK, 2 * tok)
        weights = jnp.exp(st + bias[h, :n]).reshape(rows, 2 * tok)
        vdt = dot(vp, cs, 1, 1)
        dkvs[h, :, 1] = dot(weights.astype(BF16), cs, 1, 0).astype(BF16).reshape(n, BLK, wide)
        delta = jnp.sum(weights * vdt, axis=0, keepdims=True) + jnp.sum(own * vdo, axis=0, keepdims=True)
        dst = (weights * (vdt - delta)).astype(BF16)
        dso = (own * (vdo - delta)).astype(BF16)
        dq = (dot(dst, kp, 0, 0) + dot(dso, ko, 0, 0)) * scale
        dq = jnp.where(low, dq[:tok], dq[tok:]).astype(BF16)
        gq_ref[:, c : c + wide] = dq
        dqr[h, j] = dq
        dkvs[h, :, 0] = (dot(dst, qs, 1, 0) * scale).astype(BF16).reshape(n, BLK, wide)
        for i in range(1, g):
            dq_copy(h, lax.rem(j + i, g), j).start()
        send_back(h)
        gko[:, c : c + wide] = dot(dso, qs, 1, 0) * scale

    def weight(h):
        for i in range(1, g):
            p = lax.rem(j + i, g)
            dq_copy(h, p, p).wait_recv()
        right = dqr[h].reshape(g * tok, wide)
        for i in range(1, r):
            zz = lax.rem(z + i, r)
            gs[h, zz] = dot(xr[:, zz].reshape(g * tok, w), right, 0, 0).astype(BF16)
            gw_copy(h, zz, z).start()
        gw_ref[:, h * wide : (h + 1) * wide] = dot(xr[:, z].reshape(g * tok, w), right, 0, 0)

    for h in range(pairs):
        attend(h)
        if h == 0:
            each_x(lambda p, t2: x_copy(p, t2, p, t2).wait_recv())
        else:
            weight(h - 1)
    weight(pairs - 1)

    for h in range(pairs):
        c = h * wide

        def add(d):
            back_copy(h, d, d).wait_recv()
            dk, dv = dkvr[h, d, 0].astype(F32), dkvr[h, d, 1].astype(F32)
            for b in range(bd):
                one = hot[d, b : b + 1, c : c + wide]
                gko[b * BLK : (b + 1) * BLK, c : c + wide] += dk * one
                gvo[b * BLK : (b + 1) * BLK, c : c + wide] += dv * one
        each(me + 1, n, add)
        gk_ref[:, c : c + wide] = gko[:, c : c + wide].astype(BF16)
        gv_ref[:, c : c + wide] = gvo[:, c : c + wide].astype(BF16)
        for i in range(1, r):
            zz = lax.rem(z + i, r)
            gw_copy(h, zz, zz).wait_recv()
            gw_ref[:, c : c + wide] += gr[h, zz].astype(F32)

    for h in range(pairs):
        each(me + 1, n, lambda d: kv_copy(h, d, me).wait_send())
        each(0, me, lambda o: back_copy(h, o, me).wait_send())
        for i in range(1, g):
            dq_copy(h, lax.rem(j + i, g), j).wait_send()
        for i in range(1, r):
            gw_copy(h, lax.rem(z + i, r), z).wait_send()
    each_x(lambda p, t2: x_copy(p, t2, j, t).wait_send())


def write_out(*refs):
    sems = refs[8]
    copies = [pltpu.make_async_copy(refs[i], refs[4 + i], sems.at[i]) for i in range(4)]
    for copy in copies:
        copy.start()
    for copy in copies:
        copy.wait()


def body(n, tp, g, queries, keys, values, cotangent, log_sum, chosen, normed_input):
    tok, cols = queries.shape
    wide = 2 * HD
    pairs = cols // wide
    bd = tok // BLK
    r = n // g
    w = normed_input.shape[1] // (r // tp * g)
    tiles = pltpu.VMEM((pairs, n, 2, BLK, wide), BF16)
    vmem = pl.BlockSpec(memory_space=pltpu.VMEM)
    sem = pltpu.SemaphoreType.DMA
    hbm = pl.BlockSpec(memory_space=pltpu.HBM)
    picks = chosen.transpose(2, 0, 1)
    held = [pltpu.VMEM(a.shape, a.dtype) for a in (
        queries, keys, values, cotangent, log_sum, picks, normed_input)]
    made = pl.pallas_call(
        functools.partial(kernel, n, tp, g),
        out_shape=[
            jax.ShapeDtypeStruct((tok, cols), BF16),
            jax.ShapeDtypeStruct((tok, cols), BF16),
            jax.ShapeDtypeStruct((tok, cols), BF16),
            jax.ShapeDtypeStruct((w, cols), F32),
        ],
        in_specs=[hbm] * 7,
        out_specs=[vmem] * 4,
        scratch_shapes=held + [
            sem((7,)),
            pltpu.VMEM((pairs, n + bd + 1, 1, 2 * tok), F32),
            pltpu.VMEM((n, bd, cols), F32),
            tiles, tiles, tiles, tiles,
            pltpu.VMEM((tok, cols), F32),
            pltpu.VMEM((tok, cols), F32),
            pltpu.VMEM((g, r // tp, tok, w), BF16),
            pltpu.VMEM((g, r, tok, w), BF16),
            pltpu.VMEM((pairs, g, tok, wide), BF16),
            pltpu.VMEM((pairs, r, w, wide), BF16),
            pltpu.VMEM((pairs, r, w, wide), BF16),
            sem((2, pairs, n)), sem((2, pairs, n)),
            sem((g, tp)), sem((g, tp)),
            sem((pairs, g)), sem((pairs, g)),
            sem((pairs, r)), sem((pairs, r)),
        ],
        compiler_params=pltpu.CompilerParams(has_side_effects=True, vmem_limit_bytes=67043328),
    )(queries, keys, values, cotangent, log_sum, picks, normed_input)
    return pl.pallas_call(
        write_out,
        out_shape=[jax.ShapeDtypeStruct(a.shape, a.dtype) for a in made],
        in_specs=[vmem] * 4,
        out_specs=[hbm] * 4,
        scratch_shapes=[sem((4,))],
    )(*made)


def solution(mesh):
    n, tp = mesh.shape["kv"], mesh.shape["tp"]
    g = 1
    while 4 * g * g <= n:
        g *= 2
    in_specs = (
        P("kv", "tp"), P("kv", "tp"), P("kv", "tp"), P("kv", "tp"),
        P("tp", "kv"), P("tp", None, None), P("kv", "tp"),
    )
    out_specs = (P("kv", "tp"),) * 4
    return jax.shard_map(
        functools.partial(body, n, tp, g), mesh=mesh, in_specs=in_specs, out_specs=out_specs, check_vma=False
    )
```

profile of v0, /device:TPU:16, one launch (start us, length us, event | category | flops | bytes accessed | tf_op | source)
XLA Modules:
  0.0 124.4 jit_solution(14435009240430687979)
XLA Ops:
  0.6 122.3 %shard_map.102 = (bf16[128,128]{1,0:T(8,128)(2,1)}, bf16[128,128]{1,0:T(8,128)(2,1)}, bf16[128,128]{1,0:T(8,128)(2,1)}, f32[32,128]{1,0:T(8,128)}) custom-call(bf16[128,128]{1,0:T(8,128)(2,1)} %q_in.1, bf16[128,128]{1,0:T(8,128)(2,1)} %k_in.1, bf16[128,128]{1,0:T(8,128)(2,1)} %v_in.1, bf16[128,128]{1,0:T(8,128)(2,1)} %c_in.1, f32[2,128]{1,0:T(2,128)} %lse_in.1, ...), custom_call_target="tpu_custom_call" | custom-call | tf_op jit(solution)/shard_map/pallas_call | solution.py:288
  123.0 1.5 %shard_map.103 = (bf16[128,128]{1,0:T(8,128)(2,1)}, bf16[128,128]{1,0:T(8,128)(2,1)}, bf16[128,128]{1,0:T(8,128)(2,1)}, f32[32,128]{1,0:T(8,128)}) custom-call(bf16[128,128]{1,0:T(8,128)(2,1)} %get-tuple-element.8.refs_0_, bf16[128,128]{1,0:T(8,128)(2,1)} %get-tuple-element.9.refs_1_, bf16[128,128]{1,0:T(8,128)(2,1)} %get-tuple-element.10.refs_2_, ...), custom_call_target="tpu_custom_call" | custom-call | tf_op jit(solution)/shard_map/pallas_call | solution.py:317
where the time goes:
time: 125 us; the launch traced here: 124 us
  Pallas kernels  124 us (99%)
    pallas_call x1, Pallas kernels, body(): pl.pallas_call(functools.partial(kernel, n, tp, g), out_shape=[jax.ShapeD...  122 us

commit v1 on v0

v1 whole, which is shorter than its diff:
```python
import functools

import jax
import jax.numpy as jnp
from jax import lax
from jax.experimental import pallas as pl
from jax.experimental.pallas import tpu as pltpu
from jax.sharding import PartitionSpec as P

HD = 64
BLK = 32
MASKED = -1e30
MESH = pl.DeviceIdType.MESH
F32 = jnp.float32
BF16 = jnp.bfloat16


def dot(a, b, ca, cb):
    return lax.dot_general(a, b, (((ca,), (cb,)), ((), ())), preferred_element_type=F32)


def iota(shape, dim):
    return lax.broadcasted_iota(jnp.int32, shape, dim)


def each(low, high, fn):
    def step(i, carry):
        fn(i)
        return carry
    lax.fori_loop(low, high, step, 0)


def kernel(
    g, r, tp, q_in, k_in, v_in, c_in, lse_in, pick_in, x_in,
    gq_ref, gk_ref, gv_ref, gw_ref,
    q_ref, k_ref, v_ref, c_ref, lse_ref, pick_ref, x_ref, insem,
    qs, cs, hot, bias, kz, kvs, kvt, wts, vds, back_s, back_r, rel_s, rel_r, gko, gvo, dqa,
    xs, xg, xr, dqr, gs, gr,
    zs_sem, zr_sem, ys_sem, yr_sem, bs_sem, br_sem, rs_sem, rr_sem,
    x1s, x1r, x2s, x2r, dqs_sem, dqr_sem, gs_sem, gr_sem,
):
    tok, cols = q_ref.shape
    sel, heads, blocks = pick_ref.shape
    bd = tok // BLK
    wide = 2 * tok
    chunk = g * BLK
    scale = HD ** (-0.5)
    me, t = lax.axis_index("kv"), lax.axis_index("tp")
    z, y = me // g, lax.rem(me, g)

    loads = {}
    for i, (a, b) in enumerate((
        (pick_in, pick_ref), (k_in, k_ref), (v_in, v_ref), (x_in, x_ref),
        (q_in, q_ref), (c_in, c_ref), (lse_in, lse_ref),
    )):
        loads[i] = pltpu.make_async_copy(a, b, insem.at[i])
        loads[i].start()

    barrier = pltpu.get_barrier_semaphore()

    def greet(kv, tt):
        pl.semaphore_signal(barrier, inc=1, device_id=(kv, tt), device_id_type=MESH)

    for i in range(1, r):
        greet(lax.rem(z + i, r) * g + y, t)
    for i in range(1, g):
        greet(z * g + lax.rem(y + i, g), t)
    for i in range(1, tp):
        greet(me, lax.rem(t + i, tp))
    for i in range(r):
        zz = lax.rem(z + i, r)
        if i == 0:
            @pl.when(t != z)
            def _():
                greet(zz * g + y, z)
        else:
            greet(zz * g + y, z)

    def z_copy(c, zz, slot):
        return pltpu.make_async_remote_copy(
            src_ref=(k_ref, v_ref)[c], dst_ref=kz.at[slot, c], send_sem=zs_sem.at[c, zz],
            recv_sem=zr_sem.at[c, slot], device_id=(zz * g + y, t), device_id_type=MESH)

    def y_copy(zz, yy, slot):
        return pltpu.make_async_remote_copy(
            src_ref=kvs.at[zz, yy], dst_ref=kvt.at[zz * g + slot], send_sem=ys_sem.at[zz, yy],
            recv_sem=yr_sem.at[zz, slot], device_id=(z * g + yy, t), device_id_type=MESH)

    def back_copy(c, zz, yy, slot):
        return pltpu.make_async_remote_copy(
            src_ref=back_s.at[c, zz, yy], dst_ref=back_r.at[c, zz, slot], send_sem=bs_sem.at[c, zz, yy],
            recv_sem=br_sem.at[c, zz, slot], device_id=(z * g + yy, t), device_id_type=MESH)

    def rel_copy(c, zz, slot):
        return pltpu.make_async_remote_copy(
            src_ref=rel_s.at[c, zz], dst_ref=rel_r.at[c, slot], send_sem=rs_sem.at[c, zz],
            recv_sem=rr_sem.at[c, slot], device_id=(zz * g + y, t), device_id_type=MESH)

    def x1_copy(s, slot):
        return pltpu.make_async_remote_copy(
            src_ref=xs.at[s], dst_ref=xg.at[slot], send_sem=x1s.at[s], recv_sem=x1r.at[slot],
            device_id=(t * g + y, s), device_id_type=MESH)

    def x2_copy(tt, slot):
        return pltpu.make_async_remote_copy(
            src_ref=xg, dst_ref=xr.at[slot], send_sem=x2s.at[tt], recv_sem=x2r.at[slot],
            device_id=(me, tt), device_id_type=MESH)

    def dq_copy(zz, slot):
        return pltpu.make_async_remote_copy(
            src_ref=dqr.at[z], dst_ref=dqr.at[slot], send_sem=dqs_sem.at[zz], recv_sem=dqr_sem.at[slot],
            device_id=(zz * g + y, t), device_id_type=MESH)

    def gw_copy(yy, slot):
        return pltpu.make_async_remote_copy(
            src_ref=gs.at[yy], dst_ref=gr.at[slot], send_sem=gs_sem.at[yy], recv_sem=gr_sem.at[slot],
            device_id=(z * g + yy, t), device_id_type=MESH)

    def each_x1(low, fn):
        def step(s):
            @pl.when((t != z) | (s != t))
            def _():
                fn(s)
        each(low, tp, step)

    def each_x1_in(fn):
        def step(zz):
            @pl.when((t != z) | (zz != z))
            def _():
                fn(zz)
        each(0, r, step)

    loads[0].wait()
    row_of = iota((blocks, heads * g * bd), 0) - z * (g * bd)
    col_of = iota((blocks, heads * g * bd), 1)
    at_row = lax.rem(col_of, g * bd) == row_of
    at_tok = me * bd + lax.rem(iota((blocks, heads * tok), 1), tok) // BLK == iota((blocks, heads * tok), 0)
    tok_head = iota((blocks, heads * tok), 1) // tok
    row_ids, ids = None, None
    for h in range(heads):
        mine = pick_ref[:, h, :].astype(F32).astype(BF16)
        pick_row = (at_row & (col_of // (g * bd) == h)).astype(F32).astype(BF16)
        pick_tok = (at_tok & (tok_head == h)).astype(F32).astype(BF16)
        a, b = dot(mine, pick_row, 1, 0), dot(mine, pick_tok, 1, 0)
        row_ids = a if row_ids is None else row_ids + a
        ids = b if ids is None else ids + b
    row_ids = (row_ids + 0.5).astype(jnp.int32)
    ids = (ids + 0.5).astype(jnp.int32)
    ids = jnp.where(ids < me * bd + lax.rem(iota(ids.shape, 1), tok) // BLK, ids, blocks)
    target_at = iota((r * bd, heads * g * bd), 0)
    target = (target_at // bd * g + y) * bd + lax.rem(target_at, bd)
    hit = jnp.zeros(target.shape, F32)
    for s in range(sel):
        hit = jnp.where(row_ids[s : s + 1, :] == target, 1.0, hit)
    out_at, out_from = iota((heads * g * bd, g * cols), 1), iota((heads * g * bd, g * cols), 0)
    fan = (lax.rem(out_from, g * bd) // bd == out_at // cols) & (
        lax.rem(out_at, cols) // HD == out_from // (g * bd))
    taken = dot(hit.astype(BF16), fan.astype(F32).astype(BF16), 1, 0)
    taken = jnp.where(taken > 0.5, 1.0, 0.0).reshape(r, bd, g * cols)
    for yy in range(g):
        hot[:, yy] = taken[:, :, yy * cols : (yy + 1) * cols]

    loads[1].wait()
    loads[2].wait()
    pl.semaphore_wait(barrier, (r - 1) + (g - 1) + (tp - 1) + r - jnp.where(t == z, 1, 0))

    def span(i):
        zz = r - 1 - i
        z_copy(0, zz, z).start()
        z_copy(1, zz, z).start()
    each(0, r - 1 - z, span)

    def mask(zz, yy, b):
        return jnp.broadcast_to(hot[zz, yy, pl.ds(b, 1), :], (BLK, cols))

    def picked(zz, yy, k_from, v_from):
        k_out, v_out = None, None
        for b in range(bd):
            one = mask(zz, yy, b).astype(BF16)
            k_term, v_term = k_from(b) * one, v_from(b) * one
            k_out = k_term if k_out is None else k_out + k_term
            v_out = v_term if v_out is None else v_out + v_term
        return k_out, v_out

    def own_rows(i):
        yy = y + 1 + i
        a, b = picked(z, yy, lambda b: k_ref[b * BLK : (b + 1) * BLK, :], lambda b: v_ref[b * BLK : (b + 1) * BLK, :])
        kvs[z, yy, 0] = a
        kvs[z, yy, 1] = b
        y_copy(z, yy, y).start()
    each(0, g - 1 - y, own_rows)

    loads[3].wait()
    width = x_ref.shape[1]
    w = width // tp
    eye = (iota((width, width), 0) == iota((width, width), 1)).astype(F32).astype(BF16)
    flipped = dot(eye, x_ref[...], 1, 1).astype(BF16)
    xs[...] = flipped.reshape(tp, w, tok)
    each_x1(0, lambda s: x1_copy(s, z).start())

    @pl.when(t == z)
    def _():
        xg[z] = xs[t]

    def clear(yy):
        kvt[z * g + yy] = jnp.zeros(kvt.shape[1:], BF16)
    each(y, g, clear)

    for i in (4, 5, 6):
        loads[i].wait()
    less = jnp.concatenate([-lse_ref[h : h + 1, :] for h in range(heads)], axis=1)
    owner = ids // bd
    for zz in range(r):
        need = jnp.zeros((g, wide), jnp.bool_)
        at = zz * g + iota((g, wide), 0)
        for s in range(sel):
            need = need | (owner[s : s + 1, :] == at)
        bias[zz] = jnp.where(need & (at < me), less, MASKED)
    low = iota((tok, cols), 1) < HD

    def stacked(ref):
        part = ref[...]
        zero = jnp.zeros_like(part)
        return jnp.concatenate([jnp.where(low, part, zero), jnp.where(low, zero, part)], axis=0)

    qs[...] = stacked(q_ref)
    cs[...] = stacked(c_ref)

    def relay(i):
        zz = z - 1 - i
        z_copy(0, zz, zz).wait_recv()
        z_copy(1, zz, zz).wait_recv()

        def one(k):
            yy = lax.rem(y + k, g)
            a, b = picked(zz, yy, lambda b: kz[zz, 0, b * BLK : (b + 1) * BLK, :],
                          lambda b: kz[zz, 1, b * BLK : (b + 1) * BLK, :])

            @pl.when(k != g)
            def _():
                kvs[zz, yy, 0] = a
                kvs[zz, yy, 1] = b
                y_copy(zz, yy, y).start()

            @pl.when(k == g)
            def _():
                kvt[zz * g + y, 0] = a
                kvt[zz * g + y, 1] = b
        each(1, g + 1, one)
    each(0, z, relay)

    each_x1_in(lambda zz: x1_copy(0, zz).wait_recv())
    for i in range(1, tp):
        x2_copy(lax.rem(t + i, tp), t).start()
    xr[t] = xg[...]

    key_at = iota((tok, wide), 0)
    query_at = lax.rem(iota((tok, wide), 1), tok)
    own_block = key_at // BLK
    need = jnp.zeros((tok, wide), jnp.bool_)
    own_ids = jnp.where(owner == me, lax.rem(ids, bd), bd)
    for s in range(sel):
        need = need | (own_ids[s : s + 1, :] == own_block)
    need = need | ((own_block == query_at // BLK) & (key_at <= query_at))
    own = jnp.exp(dot(k_ref[...], qs[...], 1, 1) * scale + jnp.where(need, less, MASKED))
    vdo = dot(v_ref[...], cs[...], 1, 1)
    gvo[...] = dot(own.astype(BF16), cs[...], 1, 0)
    first = jnp.sum(own * vdo, axis=0, keepdims=True)

    def send_back(c, zz):
        def one(k):
            yy = lax.rem(y + k, g)

            @pl.when((zz < z) | (yy < y))
            def _():
                back_copy(c, zz, yy, y).start()
        each(1, g, one)

    def pass_one(i, delta):
        zz = z - i

        def arrive(k):
            yy = lax.rem(y + k, g)

            @pl.when((zz < z) | (yy < y))
            def _():
                y_copy(zz, 0, yy).wait_recv()
        each(1, g, arrive)
        kp = kvt[pl.ds(zz * g, g), 0].reshape(chunk, cols)
        vp = kvt[pl.ds(zz * g, g), 1].reshape(chunk, cols)
        line = jnp.concatenate(
            [jnp.broadcast_to(bias[zz, a : a + 1, :], (BLK, wide)) for a in range(g)], axis=0)
        weights = jnp.exp(dot(kp, qs[...], 1, 1) * scale + line)
        vd = dot(vp, cs[...], 1, 1)
        wts[zz] = weights
        vds[zz] = vd
        back_s[1, zz] = dot(weights.astype(BF16), cs[...], 1, 0).astype(BF16).reshape(g, BLK, cols)
        send_back(1, zz)
        return delta + jnp.sum(weights * vd, axis=0, keepdims=True)
    delta = lax.fori_loop(0, z + 1, pass_one, first)

    dso = (own * (vdo - delta)).astype(BF16)
    dqa[...] = dot(dso, k_ref[...], 0, 0)

    def pass_two(i):
        zz = z - i
        kp = kvt[pl.ds(zz * g, g), 0].reshape(chunk, cols)
        ds = (wts[zz] * (vds[zz] - delta)).astype(BF16)
        dqa[...] += dot(ds, kp, 0, 0)
        back_s[0, zz] = (dot(ds, qs[...], 1, 0) * scale).astype(BF16).reshape(g, BLK, cols)
        send_back(0, zz)
    each(0, z + 1, pass_two)

    dq = jnp.where(low, dqa[:tok], dqa[tok:]) * scale
    dq = dq.astype(BF16)
    gq_ref[...] = dq
    dqr[z] = dq
    for i in range(1, r):
        dq_copy(lax.rem(z + i, r), z).start()
    gko[...] = dot(dso, qs[...], 1, 0) * scale

    def relay_back(c):
        own_sum = gko if c == 0 else gvo

        def own_add(i):
            yy = y + 1 + i
            back_copy(c, z, 0, yy).wait_recv()
            got = back_r[c, z, yy].astype(F32)
            for b in range(bd):
                own_sum[b * BLK : (b + 1) * BLK, :] += got * mask(z, yy, b)

        def one(i):
            zz = z - 1 - i
            sums = [back_s[c, zz, y].astype(F32) * mask(zz, y, b) for b in range(bd)]

            def add(k, acc):
                yy = lax.rem(y + k, g)
                back_copy(c, zz, 0, yy).wait_recv()
                got = back_r[c, zz, yy].astype(F32)
                return tuple(acc[b] + got * mask(zz, yy, b) for b in range(bd))
            sums = lax.fori_loop(1, g, add, tuple(sums))
            for b in range(bd):
                rel_s[c, zz, b * BLK : (b + 1) * BLK, :] = sums[b].astype(BF16)
            rel_copy(c, zz, z).start()
        each(0, z, one)
        each(0, g - 1 - y, own_add)

    relay_back(1)

    for i in range(1, tp):
        tt = lax.rem(t + i, tp)
        x2_copy(tt, tt).wait_recv()
    total = None
    for zz in range(r):
        @pl.when(zz != z)
        def _():
            dq_copy(zz, zz).wait_recv()
        part = dot(xr[:, zz].reshape(width, tok), dqr[zz], 1, 0)
        total = part if total is None else total + part
    for yy in range(g):
        gs[yy] = total[yy * w : (yy + 1) * w].astype(BF16)

        @pl.when(yy == y)
        def _():
            gw_ref[...] = total[yy * w : (yy + 1) * w]
    for i in range(1, g):
        gw_copy(lax.rem(y + i, g), y).start()

    relay_back(0)

    for i in range(1, g):
        yy = lax.rem(y + i, g)
        gw_copy(yy, yy).wait_recv()
        gw_ref[...] += gr[yy].astype(F32)

    def settle(c):
        own_sum = gko if c == 0 else gvo

        def one(i):
            zz = z + 1 + i
            rel_copy(c, 0, zz).wait_recv()
            own_sum[...] += rel_r[c, zz].astype(F32)
        each(0, r - 1 - z, one)
        (gk_ref if c == 0 else gv_ref)[...] = own_sum[...].astype(BF16)
    settle(1)
    settle(0)

    def sent_span(i):
        z_copy(0, z + 1 + i, z).wait_send()
        z_copy(1, z + 1 + i, z).wait_send()
    each(0, r - 1 - z, sent_span)
    each(0, g - 1 - y, lambda i: y_copy(z, y + 1 + i, y).wait_send())

    def sent_row(zz):
        def one(k):
            yy = lax.rem(y + k, g)
            y_copy(zz, yy, y).wait_send()
        each(1, g, one)
        rel_copy(0, zz, z).wait_send()
        rel_copy(1, zz, z).wait_send()
    each(0, z, sent_row)

    def sent_back(zz):
        def one(k):
            yy = lax.rem(y + k, g)

            @pl.when((zz < z) | (yy < y))
            def _():
                back_copy(0, zz, yy, y).wait_send()
                back_copy(1, zz, yy, y).wait_send()
        each(1, g, one)
    each(0, z + 1, sent_back)
    each_x1(0, lambda s: x1_copy(s, z).wait_send())
    for i in range(1, tp):
        x2_copy(lax.rem(t + i, tp), t).wait_send()
    for i in range(1, r):
        dq_copy(lax.rem(z + i, r), z).wait_send()
    for i in range(1, g):
        gw_copy(lax.rem(y + i, g), y).wait_send()


def write_out(*refs):
    sems = refs[8]
    copies = [pltpu.make_async_copy(refs[i], refs[4 + i], sems.at[i]) for i in range(4)]
    for copy in copies:
        copy.start()
    for copy in copies:
        copy.wait()


def body(g, r, tp, queries, keys, values, cotangent, log_sum, chosen, normed_input):
    tok, cols = queries.shape
    bd = tok // BLK
    wide = 2 * tok
    w = normed_input.shape[1] // tp
    vmem = pl.BlockSpec(memory_space=pltpu.VMEM)
    sem = pltpu.SemaphoreType.DMA
    hbm = pl.BlockSpec(memory_space=pltpu.HBM)
    picks = chosen.transpose(2, 0, 1)
    held = [pltpu.VMEM(a.shape, a.dtype) for a in (
        queries, keys, values, cotangent, log_sum, picks, normed_input)]
    made = pl.pallas_call(
        functools.partial(kernel, g, r, tp),
        out_shape=[
            jax.ShapeDtypeStruct((tok, cols), BF16),
            jax.ShapeDtypeStruct((tok, cols), BF16),
            jax.ShapeDtypeStruct((tok, cols), BF16),
            jax.ShapeDtypeStruct((w, cols), F32),
        ],
        in_specs=[hbm] * 7,
        out_specs=[vmem] * 4,
        scratch_shapes=held + [
            sem((7,)),
            pltpu.VMEM((wide, cols), BF16),
            pltpu.VMEM((wide, cols), BF16),
            pltpu.VMEM((r, g, bd, cols), F32),
            pltpu.VMEM((r, g, wide), F32),
            pltpu.VMEM((r, 2, tok, cols), BF16),
            pltpu.VMEM((r, g, 2, BLK, cols), BF16),
            pltpu.VMEM((r * g, 2, BLK, cols), BF16),
            pltpu.VMEM((r, g * BLK, wide), F32),
            pltpu.VMEM((r, g * BLK, wide), F32),
            pltpu.VMEM((2, r, g, BLK, cols), BF16),
            pltpu.VMEM((2, r, g, BLK, cols), BF16),
            pltpu.VMEM((2, r, tok, cols), BF16),
            pltpu.VMEM((2, r, tok, cols), BF16),
            pltpu.VMEM((tok, cols), F32),
            pltpu.VMEM((tok, cols), F32),
            pltpu.VMEM((wide, cols), F32),
            pltpu.VMEM((tp, w, tok), BF16),
            pltpu.VMEM((r, w, tok), BF16),
            pltpu.VMEM((tp, r, w, tok), BF16),
            pltpu.VMEM((r, tok, cols), BF16),
            pltpu.VMEM((g, w, cols), BF16),
            pltpu.VMEM((g, w, cols), BF16),
            sem((2, r)), sem((2, r)),
            sem((r, g)), sem((r, g)),
            sem((2, r, g)), sem((2, r, g)),
            sem((2, r)), sem((2, r)),
            sem((tp,)), sem((r,)),
            sem((tp,)), sem((tp,)),
            sem((r,)), sem((r,)),
            sem((g,)), sem((g,)),
        ],
        compiler_params=pltpu.CompilerParams(
            has_side_effects=True, collective_id=0, vmem_limit_bytes=67043328),
    )(queries, keys, values, cotangent, log_sum, picks, normed_input)
    return pl.pallas_call(
        write_out,
        out_shape=[jax.ShapeDtypeStruct(a.shape, a.dtype) for a in made],
        in_specs=[vmem] * 4,
        out_specs=[hbm] * 4,
        scratch_shapes=[sem((4,))],
    )(*made)


def solution(mesh):
    n, tp = mesh.shape["kv"], mesh.shape["tp"]
    g = n // tp
    in_specs = (
        P("kv", "tp"), P("kv", "tp"), P("kv", "tp"), P("kv", "tp"),
        P("tp", "kv"), P("tp", None, None), P("kv", "tp"),
    )
    out_specs = (P("kv", "tp"),) * 4
    return jax.shard_map(
        functools.partial(body, g, n // g, tp), mesh=mesh, in_specs=in_specs, out_specs=out_specs, check_vma=False
    )
```

time: 125 us -> 76.1 us (0.61)
  the two profiles are of different devices: /device:TPU:16 before, /device:TPU:22 now
where the time goes in v1:
time: 76.1 us; the launch traced here: 75.9 us
  Pallas kernels  75.2 us (99%)
    pallas_call x1, Pallas kernels, body(): pl.pallas_call(functools.partial(kernel, g, r, tp), out_shape=[jax.ShapeD...  73.8 us

profile of v1, /device:TPU:22, one launch (start us, length us, event | category | flops | bytes accessed | tf_op | source)
XLA Modules:
  0.0 75.9 jit_solution(9526965411925049156)
XLA Ops:
  0.6 73.8 %shard_map.102 = (bf16[128,128]{1,0:T(8,128)(2,1)}, bf16[128,128]{1,0:T(8,128)(2,1)}, bf16[128,128]{1,0:T(8,128)(2,1)}, f32[32,128]{1,0:T(8,128)}) custom-call(bf16[128,128]{1,0:T(8,128)(2,1)} %q_in.1, bf16[128,128]{1,0:T(8,128)(2,1)} %k_in.1, bf16[128,128]{1,0:T(8,128)(2,1)} %v_in.1, bf16[128,128]{1,0:T(8,128)(2,1)} %c_in.1, f32[2,128]{1,0:T(2,128)} %lse_in.1, ...), custom_call_target="tpu_custom_call" | custom-call | tf_op jit(solution)/shard_map/pallas_call | solution.py:442
  74.4 1.5 %shard_map.103 = (bf16[128,128]{1,0:T(8,128)(2,1)}, bf16[128,128]{1,0:T(8,128)(2,1)}, bf16[128,128]{1,0:T(8,128)(2,1)}, f32[32,128]{1,0:T(8,128)}) custom-call(bf16[128,128]{1,0:T(8,128)(2,1)} %get-tuple-element.8.refs_0_, bf16[128,128]{1,0:T(8,128)(2,1)} %get-tuple-element.9.refs_1_, bf16[128,128]{1,0:T(8,128)(2,1)} %get-tuple-element.10.refs_2_, ...), custom_call_target="tpu_custom_call" | custom-call | tf_op jit(solution)/shard_map/pallas_call | solution.py:488

commit v2 on v1

--- a/solution.py
+++ b/solution.py
@@ -35,9 +35,10 @@
     gq_ref, gk_ref, gv_ref, gw_ref,
     q_ref, k_ref, v_ref, c_ref, lse_ref, pick_ref, x_ref, insem,
     qs, cs, hot, bias, kz, kvs, kvt, wts, vds, back_s, back_r, rel_s, rel_r, gko, gvo, dqa,
-    xs, xg, xr, dqr, gs, gr,
+    xs, xg, xr, dqr, gs, gr, fs, ff, fb, fr,
     zs_sem, zr_sem, ys_sem, yr_sem, bs_sem, br_sem, rs_sem, rr_sem,
     x1s, x1r, x2s, x2r, dqs_sem, dqr_sem, gs_sem, gr_sem,
+    fys, fyr, fzs, fzr, fbs, fbr, frs, frr,
 ):
     tok, cols = q_ref.shape
     sel, heads, blocks = pick_ref.shape
@@ -47,6 +48,16 @@
     scale = HD ** (-0.5)
     me, t = lax.axis_index("kv"), lax.axis_index("tp")
     z, y = me // g, lax.rem(me, g)
+
+    def far_of(zz):
+        return r - 1 - lax.rem(zz, 4) // 2
+
+    def has_far(zz):
+        return (lax.rem(zz, 2) == 0) & (zz < r - 2)
+
+    def is_far(zz, to):
+        return has_far(zz) & (far_of(zz) == to)
+    far, mine_far = far_of(z), has_far(z)
 
     loads = {}
     for i, (a, b) in enumerate((
@@ -86,6 +97,26 @@
             src_ref=kvs.at[zz, yy], dst_ref=kvt.at[zz * g + slot], send_sem=ys_sem.at[zz, yy],
             recv_sem=yr_sem.at[zz, slot], device_id=(z * g + yy, t), device_id_type=MESH)
 
+    def far_y_copy(yy, slot):
+        return pltpu.make_async_remote_copy(
+            src_ref=fs.at[yy], dst_ref=ff.at[slot], send_sem=fys.at[yy], recv_sem=fyr.at[slot],
+            device_id=(z * g + yy, t), device_id_type=MESH)
+
+    def far_z_copy(slot):
+        return pltpu.make_async_remote_copy(
+            src_ref=ff, dst_ref=kvt.at[pl.ds(slot * g, g)], send_sem=fzs.at[0], recv_sem=fzr.at[slot],
+            device_id=(far * g + y, t), device_id_type=MESH)
+
+    def far_back_copy(c, zz):
+        return pltpu.make_async_remote_copy(
+            src_ref=back_s.at[c, zz], dst_ref=fb.at[c], send_sem=fbs.at[c, zz], recv_sem=fbr.at[c],
+            device_id=(zz * g + y, t), device_id_type=MESH)
+
+    def far_ret_copy(c, yy, slot):
+        return pltpu.make_async_remote_copy(
+            src_ref=fb.at[c, yy], dst_ref=fr.at[c, slot], send_sem=frs.at[c, yy], recv_sem=frr.at[c, slot],
+            device_id=(z * g + yy, t), device_id_type=MESH)
+
     def back_copy(c, zz, yy, slot):
         return pltpu.make_async_remote_copy(
             src_ref=back_s.at[c, zz, yy], dst_ref=back_r.at[c, zz, slot], send_sem=bs_sem.at[c, zz, yy],
@@ -131,34 +162,44 @@
         each(0, r, step)
 
     loads[0].wait()
-    row_of = iota((blocks, heads * g * bd), 0) - z * (g * bd)
+    block_of = iota((blocks, heads * g * bd), 0)
     col_of = iota((blocks, heads * g * bd), 1)
-    at_row = lax.rem(col_of, g * bd) == row_of
+    at_row = lax.rem(col_of, g * bd) == block_of - z * (g * bd)
+    at_far = lax.rem(col_of, g * bd) == block_of - far * (g * bd)
     at_tok = me * bd + lax.rem(iota((blocks, heads * tok), 1), tok) // BLK == iota((blocks, heads * tok), 0)
     tok_head = iota((blocks, heads * tok), 1) // tok
-    row_ids, ids = None, None
+    row_ids, far_ids, ids = None, None, None
     for h in range(heads):
         mine = pick_ref[:, h, :].astype(F32).astype(BF16)
         pick_row = (at_row & (col_of // (g * bd) == h)).astype(F32).astype(BF16)
+        pick_far = (at_far & (col_of // (g * bd) == h)).astype(F32).astype(BF16)
         pick_tok = (at_tok & (tok_head == h)).astype(F32).astype(BF16)
-        a, b = dot(mine, pick_row, 1, 0), dot(mine, pick_tok, 1, 0)
+        a, b, f = dot(mine, pick_row, 1, 0), dot(mine, pick_tok, 1, 0), dot(mine, pick_far, 1, 0)
+        far_ids = f if far_ids is None else far_ids + f
         row_ids = a if row_ids is None else row_ids + a
         ids = b if ids is None else ids + b
     row_ids = (row_ids + 0.5).astype(jnp.int32)
+    far_ids = (far_ids + 0.5).astype(jnp.int32)
     ids = (ids + 0.5).astype(jnp.int32)
     ids = jnp.where(ids < me * bd + lax.rem(iota(ids.shape, 1), tok) // BLK, ids, blocks)
     target_at = iota((r * bd, heads * g * bd), 0)
     target = (target_at // bd * g + y) * bd + lax.rem(target_at, bd)
     hit = jnp.zeros(target.shape, F32)
+    own_target = me * bd + iota((2 * bd, heads * g * bd), 0)
+    far_hit = jnp.zeros(own_target.shape, F32)
     for s in range(sel):
         hit = jnp.where(row_ids[s : s + 1, :] == target, 1.0, hit)
+        far_hit = jnp.where(far_ids[s : s + 1, :] == own_target, 1.0, far_hit)
     out_at, out_from = iota((heads * g * bd, g * cols), 1), iota((heads * g * bd, g * cols), 0)
     fan = (lax.rem(out_from, g * bd) // bd == out_at // cols) & (
         lax.rem(out_at, cols) // HD == out_from // (g * bd))
-    taken = dot(hit.astype(BF16), fan.astype(F32).astype(BF16), 1, 0)
+    fan = fan.astype(F32).astype(BF16)
+    far_taken = jnp.where(dot(far_hit.astype(BF16), fan, 1, 0) > 0.5, 1.0, 0.0)
+    taken = dot(hit.astype(BF16), fan, 1, 0)
     taken = jnp.where(taken > 0.5, 1.0, 0.0).reshape(r, bd, g * cols)
     for yy in range(g):
-        hot[:, yy] = taken[:, :, yy * cols : (yy + 1) * cols]
+        hot[:r, yy] = taken[:, :, yy * cols : (yy + 1) * cols]
+        hot[r, yy] = far_taken[:bd, yy * cols : (yy + 1) * cols]
 
     loads[1].wait()
     loads[2].wait()
@@ -166,8 +207,11 @@
 
     def span(i):
         zz = r - 1 - i
-        z_copy(0, zz, z).start()
-        z_copy(1, zz, z).start()
+
+        @pl.when(~is_far(z, zz))
+        def _():
+            z_copy(0, zz, z).start()
+            z_copy(1, zz, z).start()
     each(0, r - 1 - z, span)
 
     def mask(zz, yy, b):
@@ -182,9 +226,30 @@
             v_out = v_term if v_out is None else v_out + v_term
         return k_out, v_out
 
+    def own_picked(zz, yy):
+        return picked(zz, yy, lambda b: k_ref[b * BLK : (b + 1) * BLK, :], lambda b: v_ref[b * BLK : (b + 1) * BLK, :])
+
+    @pl.when(mine_far)
+    def _():
+        def one(k):
+            yy = lax.rem(y + k, g)
+            a, b = own_picked(r, yy)
+
+            @pl.when(k != g)
+            def _():
+                fs[yy, 0] = a
+                fs[yy, 1] = b
+                far_y_copy(yy, y).start()
+
+            @pl.when(k == g)
+            def _():
+                ff[y, 0] = a
+                ff[y, 1] = b
+        each(1, g + 1, one)
+
     def own_rows(i):
         yy = y + 1 + i
-        a, b = picked(z, yy, lambda b: k_ref[b * BLK : (b + 1) * BLK, :], lambda b: v_ref[b * BLK : (b + 1) * BLK, :])
+        a, b = own_picked(z, yy)
         kvs[z, yy, 0] = a
         kvs[z, yy, 1] = b
         y_copy(z, yy, y).start()
@@ -226,33 +291,11 @@
     qs[...] = stacked(q_ref)
     cs[...] = stacked(c_ref)
 
-    def relay(i):
-        zz = z - 1 - i
-        z_copy(0, zz, zz).wait_recv()
-        z_copy(1, zz, zz).wait_recv()
-
-        def one(k):
-            yy = lax.rem(y + k, g)
-            a, b = picked(zz, yy, lambda b: kz[zz, 0, b * BLK : (b + 1) * BLK, :],
-                          lambda b: kz[zz, 1, b * BLK : (b + 1) * BLK, :])
-
-            @pl.when(k != g)
-            def _():
-                kvs[zz, yy, 0] = a
-                kvs[zz, yy, 1] = b
-                y_copy(zz, yy, y).start()
-
-            @pl.when(k == g)
-            def _():
-                kvt[zz * g + y, 0] = a
-                kvt[zz * g + y, 1] = b
-        each(1, g + 1, one)
-    each(0, z, relay)
-
-    each_x1_in(lambda zz: x1_copy(0, zz).wait_recv())
-    for i in range(1, tp):
-        x2_copy(lax.rem(t + i, tp), t).start()
-    xr[t] = xg[...]
+    @pl.when(mine_far)
+    def _():
+        for i in range(1, g):
+            far_y_copy(0, lax.rem(y + i, g)).wait_recv()
+        far_z_copy(z).start()
 
     key_at = iota((tok, wide), 0)
     query_at = lax.rem(iota((tok, wide), 1), tok)
@@ -267,6 +310,37 @@
     gvo[...] = dot(own.astype(BF16), cs[...], 1, 0)
     first = jnp.sum(own * vdo, axis=0, keepdims=True)
 
+    def relay(i):
+        zz = z - 1 - i
+
+        @pl.when(~is_far(zz, z))
+        def _():
+            z_copy(0, zz, zz).wait_recv()
+            z_copy(1, zz, zz).wait_recv()
+
+            def one(k):
+                yy = lax.rem(y + k, g)
+                a, b = picked(zz, yy, lambda b: kz[zz, 0, b * BLK : (b + 1) * BLK, :],
+                              lambda b: kz[zz, 1, b * BLK : (b + 1) * BLK, :])
+
+                @pl.when(k != g)
+                def _():
+                    kvs[zz, yy, 0] = a
+                    kvs[zz, yy, 1] = b
+                    y_copy(zz, yy, y).start()
+
+                @pl.when(k == g)
+                def _():
+                    kvt[zz * g + y, 0] = a
+                    kvt[zz * g + y, 1] = b
+            each(1, g + 1, one)
+    each(0, z, relay)
+
+    each_x1_in(lambda zz: x1_copy(0, zz).wait_recv())
+    for i in range(1, tp):
+        x2_copy(lax.rem(t + i, tp), t).start()
+    xr[t] = xg[...]
+
     def send_back(c, zz):
         def one(k):
             yy = lax.rem(y + k, g)
@@ -274,7 +348,14 @@
             @pl.when((zz < z) | (yy < y))
             def _():
                 back_copy(c, zz, yy, y).start()
-        each(1, g, one)
+
+        @pl.when(is_far(zz, z))
+        def _():
+            far_back_copy(c, zz).start()
+
+        @pl.when(~is_far(zz, z))
+        def _():
+            each(1, g, one)
 
     def pass_one(i, delta):
         zz = z - i
@@ -285,7 +366,14 @@
             @pl.when((zz < z) | (yy < y))
             def _():
                 y_copy(zz, 0, yy).wait_recv()
-        each(1, g, arrive)
+
+        @pl.when(is_far(zz, z))
+        def _():
+            far_z_copy(zz).wait_recv()
+
+        @pl.when(~is_far(zz, z))
+        def _():
+            each(1, g, arrive)
         kp = kvt[pl.ds(zz * g, g), 0].reshape(chunk, cols)
         vp = kvt[pl.ds(zz * g, g), 1].reshape(chunk, cols)
         line = jnp.concatenate(
@@ -331,21 +419,49 @@
 
         def one(i):
             zz = z - 1 - i
-            sums = [back_s[c, zz, y].astype(F32) * mask(zz, y, b) for b in range(bd)]
-
-            def add(k, acc):
-                yy = lax.rem(y + k, g)
-                back_copy(c, zz, 0, yy).wait_recv()
-                got = back_r[c, zz, yy].astype(F32)
-                return tuple(acc[b] + got * mask(zz, yy, b) for b in range(bd))
-            sums = lax.fori_loop(1, g, add, tuple(sums))
-            for b in range(bd):
-                rel_s[c, zz, b * BLK : (b + 1) * BLK, :] = sums[b].astype(BF16)
-            rel_copy(c, zz, z).start()
+
+            @pl.when(~is_far(zz, z))
+            def _():
+                sums = [back_s[c, zz, y].astype(F32) * mask(zz, y, b) for b in range(bd)]
+
+                def add(k, acc):
+                    yy = lax.rem(y + k, g)
+                    back_copy(c, zz, 0, yy).wait_recv()
+                    got = back_r[c, zz, yy].astype(F32)
+                    return tuple(acc[b] + got * mask(zz, yy, b) for b in range(bd))
+                sums = lax.fori_loop(1, g, add, tuple(sums))
+                for b in range(bd):
+                    rel_s[c, zz, b * BLK : (b + 1) * BLK, :] = sums[b].astype(BF16)
+                rel_copy(c, zz, z).start()
         each(0, z, one)
         each(0, g - 1 - y, own_add)
 
+    def far_forward(c):
+        @pl.when(mine_far)
+        def _():
+            far_back_copy(c, 0).wait_recv()
+            for i in range(1, g):
+                far_ret_copy(c, lax.rem(y + i, g), y).start()
+
+    def far_add(c):
+        own_sum = gko if c == 0 else gvo
+
+        def take(got, yy):
+            for b in range(bd):
+                own_sum[b * BLK : (b + 1) * BLK, :] += got.astype(F32) * mask(r, yy, b)
+
+        @pl.when(mine_far)
+        def _():
+            take(fb[c, y], y)
+
+            def one(k):
+                yy = lax.rem(y + k, g)
+                far_ret_copy(c, 0, yy).wait_recv()
+                take(fr[c, yy], yy)
+            each(1, g, one)
+
     relay_back(1)
+    far_forward(1)
 
     for i in range(1, tp):
         tt = lax.rem(t + i, tp)
@@ -367,6 +483,9 @@
         gw_copy(lax.rem(y + i, g), y).start()
 
     relay_back(0)
+    far_forward(0)
+    far_add(1)
+    far_add(0)
 
     for i in range(1, g):
         yy = lax.rem(y + i, g)
@@ -378,16 +497,30 @@
 
         def one(i):
             zz = z + 1 + i
-            rel_copy(c, 0, zz).wait_recv()
-            own_sum[...] += rel_r[c, zz].astype(F32)
+
+            @pl.when(~is_far(z, zz))
+            def _():
+                rel_copy(c, 0, zz).wait_recv()
+                own_sum[...] += rel_r[c, zz].astype(F32)
         each(0, r - 1 - z, one)
         (gk_ref if c == 0 else gv_ref)[...] = own_sum[...].astype(BF16)
     settle(1)
     settle(0)
 
     def sent_span(i):
-        z_copy(0, z + 1 + i, z).wait_send()
-        z_copy(1, z + 1 + i, z).wait_send()
+        @pl.when(~is_far(z, z + 1 + i))
+        def _():
+            z_copy(0, z + 1 + i, z).wait_send()
+            z_copy(1, z + 1 + i, z).wait_send()
+
+    @pl.when(mine_far)
+    def _():
+        far_z_copy(z).wait_send()
+        for i in range(1, g):
+            yy = lax.rem(y + i, g)
+            far_y_copy(yy, y).wait_send()
+            far_ret_copy(0, yy, y).wait_send()
+            far_ret_copy(1, yy, y).wait_send()
     each(0, r - 1 - z, sent_span)
     each(0, g - 1 - y, lambda i: y_copy(z, y + 1 + i, y).wait_send())
 
@@ -395,9 +528,12 @@
         def one(k):
             yy = lax.rem(y + k, g)
             y_copy(zz, yy, y).wait_send()
-        each(1, g, one)
-        rel_copy(0, zz, z).wait_send()
-        rel_copy(1, zz, z).wait_send()
+
+        @pl.when(~is_far(zz, z))
+        def _():
+            each(1, g, one)
+            rel_copy(0, zz, z).wait_send()
+            rel_copy(1, zz, z).wait_send()
     each(0, z, sent_row)
 
     def sent_back(zz):
@@ -408,7 +544,15 @@
             def _():
                 back_copy(0, zz, yy, y).wait_send()
                 back_copy(1, zz, yy, y).wait_send()
-        each(1, g, one)
+
+        @pl.when(is_far(zz, z))
+        def _():
+            far_back_copy(0, zz).wait_send()
+            far_back_copy(1, zz).wait_send()
+
+        @pl.when(~is_far(zz, z))
+        def _():
+            each(1, g, one)
     each(0, z + 1, sent_back)
     each_x1(0, lambda s: x1_copy(s, z).wait_send())
     for i in range(1, tp):
@@ -453,7 +597,7 @@
             sem((7,)),
             pltpu.VMEM((wide, cols), BF16),
             pltpu.VMEM((wide, cols), BF16),
-            pltpu.VMEM((r, g, bd, cols), F32),
+            pltpu.VMEM((r + 1, g, bd, cols), F32),
             pltpu.VMEM((r, g, wide), F32),
             pltpu.VMEM((r, 2, tok, cols), BF16),
             pltpu.VMEM((r, g, 2, BLK, cols), BF16),
@@ -473,6 +617,10 @@
             pltpu.VMEM((r, tok, cols), BF16),
             pltpu.VMEM((g, w, cols), BF16),
             pltpu.VMEM((g, w, cols), BF16),
+            pltpu.VMEM((g, 2, BLK, cols), BF16),
+            pltpu.VMEM((g, 2, BLK, cols), BF16),
+            pltpu.VMEM((2, g, BLK, cols), BF16),
+            pltpu.VMEM((2, g, BLK, cols), BF16),
             sem((2, r)), sem((2, r)),
             sem((r, g)), sem((r, g)),
             sem((2, r, g)), sem((2, r, g)),
@@ -481,6 +629,10 @@
             sem((tp,)), sem((tp,)),
             sem((r,)), sem((r,)),
             sem((g,)), sem((g,)),
+            sem((g,)), sem((g,)),
+            sem((1,)), sem((r,)),
+            sem((2, r)), sem((2,)),
+            sem((2, g)), sem((2, g)),
         ],
         compiler_params=pltpu.CompilerParams(
             has_side_effects=True, collective_id=0, vmem_limit_bytes=67043328),

time: 76.1 us -> 70.4 us (0.925)
  the two profiles are of different devices: /device:TPU:22 before, /device:TPU:12 now
where the time goes in v2:
time: 70.4 us; the launch traced here: 70.2 us
  Pallas kernels  69.5 us (99%)
    pallas_call x1, Pallas kernels, body(): pl.pallas_call(functools.partial(kernel, g, r, tp), out_shape=[jax.ShapeD...  68.1 us
    pallas_call x1, Pallas kernels, body(): pl.pallas_call(write_out, out_shape=[jax.ShapeDtypeStruct(a.shape, a.dtyp...  1.47 us

profile of v2, /device:TPU:12, one launch (start us, length us, event | category | flops | bytes accessed | tf_op | source)
XLA Modules:
  0.0 70.2 jit_solution(11727610774648182759)
XLA Ops:
  0.6 68.1 %shard_map.102 = (bf16[128,128]{1,0:T(8,128)(2,1)}, bf16[128,128]{1,0:T(8,128)(2,1)}, bf16[128,128]{1,0:T(8,128)(2,1)}, f32[32,128]{1,0:T(8,128)}) custom-call(bf16[128,128]{1,0:T(8,128)(2,1)} %q_in.1, bf16[128,128]{1,0:T(8,128)(2,1)} %k_in.1, bf16[128,128]{1,0:T(8,128)(2,1)} %v_in.1, bf16[128,128]{1,0:T(8,128)(2,1)} %c_in.1, f32[2,128]{1,0:T(2,128)} %lse_in.1, ...), custom_call_target="tpu_custom_call" | custom-call | tf_op jit(solution)/shard_map/pallas_call | solution.py:586
  68.7 1.5 %shard_map.103 = (bf16[128,128]{1,0:T(8,128)(2,1)}, bf16[128,128]{1,0:T(8,128)(2,1)}, bf16[128,128]{1,0:T(8,128)(2,1)}, f32[32,128]{1,0:T(8,128)}) custom-call(bf16[128,128]{1,0:T(8,128)(2,1)} %get-tuple-element.8.refs_0_, bf16[128,128]{1,0:T(8,128)(2,1)} %get-tuple-element.9.refs_1_, bf16[128,128]{1,0:T(8,128)(2,1)} %get-tuple-element.10.refs_2_, ...), custom_call_target="tpu_custom_call" | custom-call | tf_op jit(solution)/shard_map/pallas_call | solution.py:640

commit v3 on v2

--- a/solution.py
+++ b/solution.py
@@ -33,13 +33,14 @@
 def kernel(
     g, r, tp, q_in, k_in, v_in, c_in, lse_in, pick_in, x_in,
     gq_ref, gk_ref, gv_ref, gw_ref,
-    q_ref, k_ref, v_ref, c_ref, lse_ref, pick_ref, x_ref, insem,
+    q_ref, kv_ref, c_ref, lse_ref, pick_ref, x_ref, insem,
     qs, cs, hot, bias, kz, kvs, kvt, wts, vds, back_s, back_r, rel_s, rel_r, gko, gvo, dqa,
     xs, xg, xr, dqr, gs, gr, fs, ff, fb, fr,
     zs_sem, zr_sem, ys_sem, yr_sem, bs_sem, br_sem, rs_sem, rr_sem,
     x1s, x1r, x2s, x2r, dqs_sem, dqr_sem, gs_sem, gr_sem,
     fys, fyr, fzs, fzr, fbs, fbr, frs, frr,
 ):
+    k_ref, v_ref = kv_ref.at[0], kv_ref.at[1]
     tok, cols = q_ref.shape
     sel, heads, blocks = pick_ref.shape
     bd = tok // BLK
@@ -87,65 +88,59 @@
         else:
             greet(zz * g + y, z)
 
-    def z_copy(c, zz, slot):
+    def remote(src, dst, ssem, rsem, kv, tt):
         return pltpu.make_async_remote_copy(
-            src_ref=(k_ref, v_ref)[c], dst_ref=kz.at[slot, c], send_sem=zs_sem.at[c, zz],
-            recv_sem=zr_sem.at[c, slot], device_id=(zz * g + y, t), device_id_type=MESH)
+            src_ref=src, dst_ref=dst, send_sem=ssem, recv_sem=rsem, device_id=(kv, tt), device_id_type=MESH)
+
+    def z_copy(zz, slot):
+        return remote(kv_ref, kz.at[slot], zs_sem.at[0], zr_sem.at[slot], zz * g + y, t)
 
     def y_copy(zz, yy, slot):
-        return pltpu.make_async_remote_copy(
-            src_ref=kvs.at[zz, yy], dst_ref=kvt.at[zz * g + slot], send_sem=ys_sem.at[zz, yy],
-            recv_sem=yr_sem.at[zz, slot], device_id=(z * g + yy, t), device_id_type=MESH)
+        return remote(kvs.at[zz, yy], kvt.at[zz * g + slot], ys_sem.at[zz], yr_sem.at[zz], z * g + yy, t)
 
     def far_y_copy(yy, slot):
-        return pltpu.make_async_remote_copy(
-            src_ref=fs.at[yy], dst_ref=ff.at[slot], send_sem=fys.at[yy], recv_sem=fyr.at[slot],
-            device_id=(z * g + yy, t), device_id_type=MESH)
+        return remote(fs.at[yy], ff.at[slot], fys.at[0], fyr.at[0], z * g + yy, t)
 
     def far_z_copy(slot):
-        return pltpu.make_async_remote_copy(
-            src_ref=ff, dst_ref=kvt.at[pl.ds(slot * g, g)], send_sem=fzs.at[0], recv_sem=fzr.at[slot],
-            device_id=(far * g + y, t), device_id_type=MESH)
+        return remote(ff, kvt.at[pl.ds(slot * g, g)], fzs.at[0], fzr.at[slot // 4], far * g + y, t)
 
     def far_back_copy(c, zz):
-        return pltpu.make_async_remote_copy(
-            src_ref=back_s.at[c, zz], dst_ref=fb.at[c], send_sem=fbs.at[c, zz], recv_sem=fbr.at[c],
-            device_id=(zz * g + y, t), device_id_type=MESH)
+        return remote(back_s.at[c, zz], fb.at[c], fbs.at[c, zz // 4], fbr.at[c], zz * g + y, t)
 
     def far_ret_copy(c, yy, slot):
-        return pltpu.make_async_remote_copy(
-            src_ref=fb.at[c, yy], dst_ref=fr.at[c, slot], send_sem=frs.at[c, yy], recv_sem=frr.at[c, slot],
-            device_id=(z * g + yy, t), device_id_type=MESH)
+        return remote(fb.at[c, yy], fr.at[c, slot], frs.at[c], frr.at[c], z * g + yy, t)
 
     def back_copy(c, zz, yy, slot):
-        return pltpu.make_async_remote_copy(
-            src_ref=back_s.at[c, zz, yy], dst_ref=back_r.at[c, zz, slot], send_sem=bs_sem.at[c, zz, yy],
-            recv_sem=br_sem.at[c, zz, slot], device_id=(z * g + yy, t), device_id_type=MESH)
+        return remote(back_s.at[c, zz, yy], back_r.at[c, zz, slot], bs_sem.at[c, zz], br_sem.at[c, zz], z * g + yy, t)
 
     def rel_copy(c, zz, slot):
-        return pltpu.make_async_remote_copy(
-            src_ref=rel_s.at[c, zz], dst_ref=rel_r.at[c, slot], send_sem=rs_sem.at[c, zz],
-            recv_sem=rr_sem.at[c, slot], device_id=(zz * g + y, t), device_id_type=MESH)
+        return remote(rel_s.at[c, zz], rel_r.at[c, slot], rs_sem.at[c], rr_sem.at[c, slot], zz * g + y, t)
 
     def x1_copy(s, slot):
-        return pltpu.make_async_remote_copy(
-            src_ref=xs.at[s], dst_ref=xg.at[slot], send_sem=x1s.at[s], recv_sem=x1r.at[slot],
-            device_id=(t * g + y, s), device_id_type=MESH)
+        return remote(xs.at[s], xg.at[slot], x1s.at[0], x1r.at[0], t * g + y, s)
 
     def x2_copy(tt, slot):
-        return pltpu.make_async_remote_copy(
-            src_ref=xg, dst_ref=xr.at[slot], send_sem=x2s.at[tt], recv_sem=x2r.at[slot],
-            device_id=(me, tt), device_id_type=MESH)
+        return remote(xg, xr.at[slot], x2s.at[0], x2r.at[0], me, tt)
 
     def dq_copy(zz, slot):
-        return pltpu.make_async_remote_copy(
-            src_ref=dqr.at[z], dst_ref=dqr.at[slot], send_sem=dqs_sem.at[zz], recv_sem=dqr_sem.at[slot],
-            device_id=(zz * g + y, t), device_id_type=MESH)
+        return remote(dqr.at[z], dqr.at[slot], dqs_sem.at[0], dqr_sem.at[0], zz * g + y, t)
 
     def gw_copy(yy, slot):
-        return pltpu.make_async_remote_copy(
-            src_ref=gs.at[yy], dst_ref=gr.at[slot], send_sem=gs_sem.at[yy], recv_sem=gr_sem.at[slot],
-            device_id=(z * g + yy, t), device_id_type=MESH)
+        return remote(gs.at[yy], gr.at[slot], gs_sem.at[0], gr_sem.at[0], z * g + yy, t)
+
+    other = z * g + lax.rem(y + 1, g)
+
+    def arrived(ref, sem):
+        remote(ref, ref, sem, sem, other, t).wait_recv()
+
+    def left(ref, sem):
+        remote(ref, ref, sem, sem, other, t).wait_send()
+
+    def counted(count, most, fn):
+        for i in range(1, most + 1):
+            @pl.when(count == i)
+            def _():
+                fn(i)
 
     def each_x1(low, fn):
         def step(s):
@@ -153,13 +148,6 @@
             def _():
                 fn(s)
         each(low, tp, step)
-
-    def each_x1_in(fn):
-        def step(zz):
-            @pl.when((t != z) | (zz != z))
-            def _():
-                fn(zz)
-        each(0, r, step)
 
     loads[0].wait()
     block_of = iota((blocks, heads * g * bd), 0)
@@ -210,8 +198,7 @@
 
         @pl.when(~is_far(z, zz))
         def _():
-            z_copy(0, zz, z).start()
-            z_copy(1, zz, z).start()
+            z_copy(zz, z).start()
     each(0, r - 1 - z, span)
 
     def mask(zz, yy, b):
@@ -290,12 +277,6 @@
 
     qs[...] = stacked(q_ref)
     cs[...] = stacked(c_ref)
-
-    @pl.when(mine_far)
-    def _():
-        for i in range(1, g):
-            far_y_copy(0, lax.rem(y + i, g)).wait_recv()
-        far_z_copy(z).start()
 
     key_at = iota((tok, wide), 0)
     query_at = lax.rem(iota((tok, wide), 1), tok)
@@ -315,8 +296,7 @@
 
         @pl.when(~is_far(zz, z))
         def _():
-            z_copy(0, zz, zz).wait_recv()
-            z_copy(1, zz, zz).wait_recv()
+            z_copy(zz, zz).wait_recv()
 
             def one(k):
                 yy = lax.rem(y + k, g)
@@ -334,12 +314,14 @@
                     kvt[zz * g + y, 0] = a
                     kvt[zz * g + y, 1] = b
             each(1, g + 1, one)
-    each(0, z, relay)
-
-    each_x1_in(lambda zz: x1_copy(0, zz).wait_recv())
-    for i in range(1, tp):
-        x2_copy(lax.rem(t + i, tp), t).start()
-    xr[t] = xg[...]
+    once = jnp.minimum(z, 1)
+    each(0, once, relay)
+
+    @pl.when(mine_far)
+    def _():
+        arrived(ff.at[pl.ds(0, g - 1)], fyr.at[0])
+        far_z_copy(z).start()
+    each(once, z, relay)
 
     def send_back(c, zz):
         def one(k):
@@ -360,20 +342,17 @@
     def pass_one(i, delta):
         zz = z - i
 
-        def arrive(k):
-            yy = lax.rem(y + k, g)
-
-            @pl.when((zz < z) | (yy < y))
-            def _():
-                y_copy(zz, 0, yy).wait_recv()
-
         @pl.when(is_far(zz, z))
         def _():
             far_z_copy(zz).wait_recv()
 
-        @pl.when(~is_far(zz, z))
-        def _():
-            each(1, g, arrive)
+        @pl.when((zz < z) & ~is_far(zz, z))
+        def _():
+            arrived(kvt.at[pl.ds(zz * g, g - 1)], yr_sem.at[zz])
+
+        @pl.when(zz == z)
+        def _():
+            counted(y, g - 1, lambda i: arrived(kvt.at[pl.ds(z * g, i)], yr_sem.at[z]))
         kp = kvt[pl.ds(zz * g, g), 0].reshape(chunk, cols)
         vp = kvt[pl.ds(zz * g, g), 1].reshape(chunk, cols)
         line = jnp.concatenate(
@@ -407,12 +386,16 @@
         dq_copy(lax.rem(z + i, r), z).start()
     gko[...] = dot(dso, qs[...], 1, 0) * scale
 
+    counted(tp - jnp.where(t == z, 1, 0), tp, lambda i: arrived(xg.at[pl.ds(0, i)], x1r.at[0]))
+    for i in range(1, tp):
+        x2_copy(lax.rem(t + i, tp), t).start()
+    xr[t] = xg[...]
+
     def relay_back(c):
         own_sum = gko if c == 0 else gvo
 
         def own_add(i):
             yy = y + 1 + i
-            back_copy(c, z, 0, yy).wait_recv()
             got = back_r[c, z, yy].astype(F32)
             for b in range(bd):
                 own_sum[b * BLK : (b + 1) * BLK, :] += got * mask(z, yy, b)
@@ -422,11 +405,11 @@
 
             @pl.when(~is_far(zz, z))
             def _():
+                arrived(back_r.at[c, zz, pl.ds(0, g - 1)], br_sem.at[c, zz])
                 sums = [back_s[c, zz, y].astype(F32) * mask(zz, y, b) for b in range(bd)]
 
                 def add(k, acc):
                     yy = lax.rem(y + k, g)
-                    back_copy(c, zz, 0, yy).wait_recv()
                     got = back_r[c, zz, yy].astype(F32)
                     return tuple(acc[b] + got * mask(zz, yy, b) for b in range(bd))
                 sums = lax.fori_loop(1, g, add, tuple(sums))
@@ -434,6 +417,7 @@
                     rel_s[c, zz, b * BLK : (b + 1) * BLK, :] = sums[b].astype(BF16)
                 rel_copy(c, zz, z).start()
         each(0, z, one)
+        counted(g - 1 - y, g - 1, lambda i: arrived(back_r.at[c, z, pl.ds(0, i)], br_sem.at[c, z]))
         each(0, g - 1 - y, own_add)
 
     def far_forward(c):
@@ -453,24 +437,21 @@
         @pl.when(mine_far)
         def _():
             take(fb[c, y], y)
+            arrived(fr.at[c, pl.ds(0, g - 1)], frr.at[c])
 
             def one(k):
                 yy = lax.rem(y + k, g)
-                far_ret_copy(c, 0, yy).wait_recv()
                 take(fr[c, yy], yy)
             each(1, g, one)
 
     relay_back(1)
     far_forward(1)
-
-    for i in range(1, tp):
-        tt = lax.rem(t + i, tp)
-        x2_copy(tt, tt).wait_recv()
+    far_forward(0)
+
+    arrived(xr.at[pl.ds(0, tp - 1)], x2r.at[0])
+    arrived(dqr.at[pl.ds(0, r - 1)], dqr_sem.at[0])
     total = None
     for zz in range(r):
-        @pl.when(zz != z)
-        def _():
-            dq_copy(zz, zz).wait_recv()
         part = dot(xr[:, zz].reshape(width, tok), dqr[zz], 1, 0)
         total = part if total is None else total + part
     for yy in range(g):
@@ -483,14 +464,12 @@
         gw_copy(lax.rem(y + i, g), y).start()
 
     relay_back(0)
-    far_forward(0)
     far_add(1)
     far_add(0)
 
+    arrived(gr.at[pl.ds(0, g - 1)], gr_sem.at[0])
     for i in range(1, g):
-        yy = lax.rem(y + i, g)
-        gw_copy(yy, yy).wait_recv()
-        gw_ref[...] += gr[yy].astype(F32)
+        gw_ref[...] += gr[lax.rem(y + i, g)].astype(F32)
 
     def settle(c):
         own_sum = gko if c == 0 else gvo
@@ -507,44 +486,22 @@
     settle(1)
     settle(0)
 
-    def sent_span(i):
-        @pl.when(~is_far(z, z + 1 + i))
-        def _():
-            z_copy(0, z + 1 + i, z).wait_send()
-            z_copy(1, z + 1 + i, z).wait_send()
+    in_far = jnp.where(z == r - 1, 2, 0) + jnp.where(z == r - 2, 1, 0)
+    counted(r - 1 - z - jnp.where(mine_far, 1, 0), r - 1, lambda i: left(kz.at[pl.ds(0, i)], zs_sem.at[0]))
+    counted(g - 1 - y, g - 1, lambda i: left(kvs.at[z, pl.ds(0, i)], ys_sem.at[z]))
 
     @pl.when(mine_far)
     def _():
         far_z_copy(z).wait_send()
-        for i in range(1, g):
-            yy = lax.rem(y + i, g)
-            far_y_copy(yy, y).wait_send()
-            far_ret_copy(0, yy, y).wait_send()
-            far_ret_copy(1, yy, y).wait_send()
-    each(0, r - 1 - z, sent_span)
-    each(0, g - 1 - y, lambda i: y_copy(z, y + 1 + i, y).wait_send())
+        left(fs.at[pl.ds(0, g - 1)], fys.at[0])
+        left(fb.at[0, pl.ds(0, g - 1)], frs.at[0])
+        left(fb.at[1, pl.ds(0, g - 1)], frs.at[1])
+
+    for c in range(2):
+        counted(z - in_far, r - 1, lambda i: left(rel_s.at[c, pl.ds(0, i)], rs_sem.at[c]))
+        counted(y, g - 1, lambda i: left(back_s.at[c, z, pl.ds(0, i)], bs_sem.at[c, z]))
 
     def sent_row(zz):
-        def one(k):
-            yy = lax.rem(y + k, g)
-            y_copy(zz, yy, y).wait_send()
-
-        @pl.when(~is_far(zz, z))
-        def _():
-            each(1, g, one)
-            rel_copy(0, zz, z).wait_send()
-            rel_copy(1, zz, z).wait_send()
-    each(0, z, sent_row)
-
-    def sent_back(zz):
-        def one(k):
-            yy = lax.rem(y + k, g)
-
-            @pl.when((zz < z) | (yy < y))
-            def _():
-                back_copy(0, zz, yy, y).wait_send()
-                back_copy(1, zz, yy, y).wait_send()
-
         @pl.when(is_far(zz, z))
         def _():
             far_back_copy(0, zz).wait_send()
@@ -552,15 +509,14 @@
 
         @pl.when(~is_far(zz, z))
         def _():
-            each(1, g, one)
-    each(0, z + 1, sent_back)
-    each_x1(0, lambda s: x1_copy(s, z).wait_send())
-    for i in range(1, tp):
-        x2_copy(lax.rem(t + i, tp), t).wait_send()
-    for i in range(1, r):
-        dq_copy(lax.rem(z + i, r), z).wait_send()
-    for i in range(1, g):
-        gw_copy(lax.rem(y + i, g), y).wait_send()
+            left(kvs.at[zz, pl.ds(0, g - 1)], ys_sem.at[zz])
+            left(back_s.at[0, zz, pl.ds(0, g - 1)], bs_sem.at[0, zz])
+            left(back_s.at[1, zz, pl.ds(0, g - 1)], bs_sem.at[1, zz])
+    each(0, z, sent_row)
+    counted(tp - jnp.where(t == z, 1, 0), tp, lambda i: left(xs.at[pl.ds(0, i)], x1s.at[0]))
+    left(xr.at[pl.ds(0, tp - 1)], x2s.at[0])
+    left(dqr.at[pl.ds(0, r - 1)], dqs_sem.at[0])
+    left(gs.at[pl.ds(0, g - 1)], gs_sem.at[0])
 
 
 def write_out(*refs):
@@ -582,7 +538,7 @@
     hbm = pl.BlockSpec(memory_space=pltpu.HBM)
     picks = chosen.transpose(2, 0, 1)
     held = [pltpu.VMEM(a.shape, a.dtype) for a in (
-        queries, keys, values, cotangent, log_sum, picks, normed_input)]
+        queries, jax.ShapeDtypeStruct((2, tok, cols), BF16), cotangent, log_sum, picks, normed_input)]
     made = pl.pallas_call(
         functools.partial(kernel, g, r, tp),
         out_shape=[
@@ -621,18 +577,18 @@
             pltpu.VMEM((g, 2, BLK, cols), BF16),
             pltpu.VMEM((2, g, BLK, cols), BF16),
             pltpu.VMEM((2, g, BLK, cols), BF16),
+            sem((1,)), sem((r,)),
+            sem((r,)), sem((r,)),
             sem((2, r)), sem((2, r)),
-            sem((r, g)), sem((r, g)),
-            sem((2, r, g)), sem((2, r, g)),
-            sem((2, r)), sem((2, r)),
-            sem((tp,)), sem((r,)),
-            sem((tp,)), sem((tp,)),
-            sem((r,)), sem((r,)),
-            sem((g,)), sem((g,)),
-            sem((g,)), sem((g,)),
-            sem((1,)), sem((r,)),
-            sem((2, r)), sem((2,)),
-            sem((2, g)), sem((2, g)),
+            sem((2,)), sem((2, r)),
+            sem((1,)), sem((1,)),
+            sem((1,)), sem((1,)),
+            sem((1,)), sem((1,)),
+            sem((1,)), sem((1,)),
+            sem((1,)), sem((1,)),
+            sem((1,)), sem((2,)),
+            sem((2, 2)), sem((2,)),
+            sem((2,)), sem((2,)),
         ],
         compiler_params=pltpu.CompilerParams(
             has_side_effects=True, collective_id=0, vmem_limit_bytes=67043328),

time: 70.4 us -> 65.9 us (0.936)
  Pallas kernels: 69.5 us -> 65.1 us
    pallas_call x1, Pallas kernels: 68.1 us -> 63.6 us  [body(): pl.pallas_call(functools.partial(kernel, g, r, tp), out_shape=[jax.ShapeD...]
where the time goes in v3:
time: 65.9 us; the launch traced here: 65.7 us
  Pallas kernels  65.1 us (99%)
    pallas_call x1, Pallas kernels, body(): pl.pallas_call(functools.partial(kernel, g, r, tp), out_shape=[jax.ShapeD...  63.6 us
    pallas_call x1, Pallas kernels, body(): pl.pallas_call(write_out, out_shape=[jax.ShapeDtypeStruct(a.shape, a.dtyp...  1.47 us

profile of v3, /device:TPU:12, one launch (start us, length us, event | category | flops | bytes accessed | tf_op | source)
XLA Modules:
  0.0 65.7 jit_solution(17093980425182621618)
XLA Ops:
  0.6 63.6 %shard_map.102 = (bf16[128,128]{1,0:T(8,128)(2,1)}, bf16[128,128]{1,0:T(8,128)(2,1)}, bf16[128,128]{1,0:T(8,128)(2,1)}, f32[32,128]{1,0:T(8,128)}) custom-call(bf16[128,128]{1,0:T(8,128)(2,1)} %q_in.1, bf16[128,128]{1,0:T(8,128)(2,1)} %k_in.1, bf16[128,128]{1,0:T(8,128)(2,1)} %v_in.1, bf16[128,128]{1,0:T(8,128)(2,1)} %c_in.1, f32[2,128]{1,0:T(2,128)} %lse_in.1, ...), custom_call_target="tpu_custom_call" | custom-call | tf_op jit(solution)/shard_map/pallas_call | solution.py:542
  64.2 1.5 %shard_map.103 = (bf16[128,128]{1,0:T(8,128)(2,1)}, bf16[128,128]{1,0:T(8,128)(2,1)}, bf16[128,128]{1,0:T(8,128)(2,1)}, f32[32,128]{1,0:T(8,128)}) custom-call(bf16[128,128]{1,0:T(8,128)(2,1)} %get-tuple-element.8.refs_0_, bf16[128,128]{1,0:T(8,128)(2,1)} %get-tuple-element.9.refs_1_, bf16[128,128]{1,0:T(8,128)(2,1)} %get-tuple-element.10.refs_2_, ...), custom_call_target="tpu_custom_call" | custom-call | tf_op jit(solution)/shard_map/pallas_call | solution.py:596

commit v4 on v3

--- a/solution.py
+++ b/solution.py
@@ -30,11 +30,15 @@
     lax.fori_loop(low, high, step, 0)
 
 
+def far_first(n):
+    return sorted(range(1, n), key=lambda i: -min(i, n - i))
+
+
 def kernel(
     g, r, tp, q_in, k_in, v_in, c_in, lse_in, pick_in, x_in,
     gq_ref, gk_ref, gv_ref, gw_ref,
     q_ref, kv_ref, c_ref, lse_ref, pick_ref, x_ref, insem,
-    qs, cs, hot, bias, kz, kvs, kvt, wts, vds, back_s, back_r, rel_s, rel_r, gko, gvo, dqa,
+    qs, cs, hot, bias, kz, kvs, kvt, wts, vds, dss, back_s, back_r, rel_s, rel_r, gko, gvo, dqa,
     xs, xg, xr, dqr, gs, gr, fs, ff, fb, fr,
     zs_sem, zr_sem, ys_sem, yr_sem, bs_sem, br_sem, rs_sem, rr_sem,
     x1s, x1r, x2s, x2r, dqs_sem, dqr_sem, gs_sem, gr_sem,
@@ -58,7 +62,13 @@
 
     def is_far(zz, to):
         return has_far(zz) & (far_of(zz) == to)
-    far, mine_far = far_of(z), has_far(z)
+
+    def far_back(zz):
+        return (zz == 2) | (zz == 4)
+
+    def is_far_back(zz, to):
+        return far_back(zz) & (far_of(zz) == to)
+    far, mine_far, mine_far_back = far_of(z), has_far(z), far_back(z)
 
     loads = {}
     for i, (a, b) in enumerate((
@@ -194,7 +204,7 @@
     pl.semaphore_wait(barrier, (r - 1) + (g - 1) + (tp - 1) + r - jnp.where(t == z, 1, 0))
 
     def span(i):
-        zz = r - 1 - i
+        zz = z + 1 + i
 
         @pl.when(~is_far(z, zz))
         def _():
@@ -218,21 +228,12 @@
 
     @pl.when(mine_far)
     def _():
-        def one(k):
-            yy = lax.rem(y + k, g)
+        for yy in range(g):
             a, b = own_picked(r, yy)
-
-            @pl.when(k != g)
-            def _():
-                fs[yy, 0] = a
-                fs[yy, 1] = b
-                far_y_copy(yy, y).start()
-
-            @pl.when(k == g)
-            def _():
-                ff[y, 0] = a
-                ff[y, 1] = b
-        each(1, g + 1, one)
+            fs[yy, 0] = a
+            fs[yy, 1] = b
+        each(1, g, lambda k: far_y_copy(lax.rem(y + k, g), y).start())
+        ff[y] = fs[y]
 
     def own_rows(i):
         yy = y + 1 + i
@@ -298,22 +299,13 @@
         def _():
             z_copy(zz, zz).wait_recv()
 
-            def one(k):
-                yy = lax.rem(y + k, g)
+            for yy in range(g):
                 a, b = picked(zz, yy, lambda b: kz[zz, 0, b * BLK : (b + 1) * BLK, :],
                               lambda b: kz[zz, 1, b * BLK : (b + 1) * BLK, :])
-
-                @pl.when(k != g)
-                def _():
-                    kvs[zz, yy, 0] = a
-                    kvs[zz, yy, 1] = b
-                    y_copy(zz, yy, y).start()
-
-                @pl.when(k == g)
-                def _():
-                    kvt[zz * g + y, 0] = a
-                    kvt[zz * g + y, 1] = b
-            each(1, g + 1, one)
+                kvs[zz, yy, 0] = a
+                kvs[zz, yy, 1] = b
+            each(1, g, lambda k: y_copy(zz, lax.rem(y + k, g), y).start())
+            kvt[zz * g + y] = kvs[zz, y]
     once = jnp.minimum(z, 1)
     each(0, once, relay)
 
@@ -331,13 +323,14 @@
             def _():
                 back_copy(c, zz, yy, y).start()
 
-        @pl.when(is_far(zz, z))
+        @pl.when(is_far_back(zz, z))
         def _():
             far_back_copy(c, zz).start()
 
-        @pl.when(~is_far(zz, z))
+        @pl.when(~is_far_back(zz, z))
         def _():
             each(1, g, one)
+            back_r[c, zz, y] = back_s[c, zz, y]
 
     def pass_one(i, delta):
         zz = z - i
@@ -364,34 +357,48 @@
         back_s[1, zz] = dot(weights.astype(BF16), cs[...], 1, 0).astype(BF16).reshape(g, BLK, cols)
         send_back(1, zz)
         return delta + jnp.sum(weights * vd, axis=0, keepdims=True)
-    delta = lax.fori_loop(0, z + 1, pass_one, first)
+    middle = (z + 2) // 2
+    delta = lax.fori_loop(0, middle, pass_one, first)
+
+    counted(tp - jnp.where(t == z, 1, 0), tp, lambda i: arrived(xg.at[pl.ds(0, i)], x1r.at[0]))
+    for i in range(1, tp):
+        x2_copy(lax.rem(t + i, tp), t).start()
+    xr[t] = xg[...]
+    delta = lax.fori_loop(middle, z + 1, pass_one, delta)
 
     dso = (own * (vdo - delta)).astype(BF16)
     dqa[...] = dot(dso, k_ref[...], 0, 0)
 
-    def pass_two(i):
-        zz = z - i
+    def key_grads(zz):
+        back_s[0, zz] = (dot(dss[zz], qs[...], 1, 0) * scale).astype(BF16).reshape(g, BLK, cols)
+        send_back(0, zz)
+
+    def pass_two(zz):
         kp = kvt[pl.ds(zz * g, g), 0].reshape(chunk, cols)
         ds = (wts[zz] * (vds[zz] - delta)).astype(BF16)
+        dss[zz] = ds
         dqa[...] += dot(ds, kp, 0, 0)
-        back_s[0, zz] = (dot(ds, qs[...], 1, 0) * scale).astype(BF16).reshape(g, BLK, cols)
-        send_back(0, zz)
+
+        @pl.when(is_far_back(zz, z))
+        def _():
+            key_grads(zz)
     each(0, z + 1, pass_two)
 
     dq = jnp.where(low, dqa[:tok], dqa[tok:]) * scale
     dq = dq.astype(BF16)
     gq_ref[...] = dq
     dqr[z] = dq
-    for i in range(1, r):
+    for i in far_first(r):
         dq_copy(lax.rem(z + i, r), z).start()
+
+    def other_key_grads(zz):
+        @pl.when(~is_far_back(zz, z))
+        def _():
+            key_grads(zz)
+    each(0, z + 1, other_key_grads)
     gko[...] = dot(dso, qs[...], 1, 0) * scale
 
-    counted(tp - jnp.where(t == z, 1, 0), tp, lambda i: arrived(xg.at[pl.ds(0, i)], x1r.at[0]))
-    for i in range(1, tp):
-        x2_copy(lax.rem(t + i, tp), t).start()
-    xr[t] = xg[...]
-
-    def relay_back(c):
+    def relay_back(c, low_z, high_z, with_own):
         own_sum = gko if c == 0 else gvo
 
         def own_add(i):
@@ -401,27 +408,27 @@
                 own_sum[b * BLK : (b + 1) * BLK, :] += got * mask(z, yy, b)
 
         def one(i):
-            zz = z - 1 - i
-
-            @pl.when(~is_far(zz, z))
+            zz = i if c == 0 else z - 1 - i
+
+            @pl.when(~is_far_back(zz, z))
             def _():
                 arrived(back_r.at[c, zz, pl.ds(0, g - 1)], br_sem.at[c, zz])
-                sums = [back_s[c, zz, y].astype(F32) * mask(zz, y, b) for b in range(bd)]
-
-                def add(k, acc):
-                    yy = lax.rem(y + k, g)
+                sums = [None] * bd
+                for yy in range(g):
                     got = back_r[c, zz, yy].astype(F32)
-                    return tuple(acc[b] + got * mask(zz, yy, b) for b in range(bd))
-                sums = lax.fori_loop(1, g, add, tuple(sums))
+                    for b in range(bd):
+                        term = got * mask(zz, yy, b)
+                        sums[b] = term if sums[b] is None else sums[b] + term
                 for b in range(bd):
                     rel_s[c, zz, b * BLK : (b + 1) * BLK, :] = sums[b].astype(BF16)
                 rel_copy(c, zz, z).start()
-        each(0, z, one)
-        counted(g - 1 - y, g - 1, lambda i: arrived(back_r.at[c, z, pl.ds(0, i)], br_sem.at[c, z]))
-        each(0, g - 1 - y, own_add)
+        each(low_z, high_z, one)
+        if with_own:
+            counted(g - 1 - y, g - 1, lambda i: arrived(back_r.at[c, z, pl.ds(0, i)], br_sem.at[c, z]))
+            each(0, g - 1 - y, own_add)
 
     def far_forward(c):
-        @pl.when(mine_far)
+        @pl.when(mine_far_back)
         def _():
             far_back_copy(c, 0).wait_recv()
             for i in range(1, g):
@@ -430,23 +437,23 @@
     def far_add(c):
         own_sum = gko if c == 0 else gvo
 
-        def take(got, yy):
+        @pl.when(mine_far_back)
+        def _():
+            arrived(fr.at[c, pl.ds(0, g - 1)], frr.at[c])
+            fr[c, y] = fb[c, y]
+            sums = [own_sum[b * BLK : (b + 1) * BLK, :] for b in range(bd)]
+            for yy in range(g):
+                got = fr[c, yy].astype(F32)
+                for b in range(bd):
+                    sums[b] = sums[b] + got * mask(r, yy, b)
             for b in range(bd):
-                own_sum[b * BLK : (b + 1) * BLK, :] += got.astype(F32) * mask(r, yy, b)
-
-        @pl.when(mine_far)
-        def _():
-            take(fb[c, y], y)
-            arrived(fr.at[c, pl.ds(0, g - 1)], frr.at[c])
-
-            def one(k):
-                yy = lax.rem(y + k, g)
-                take(fr[c, yy], yy)
-            each(1, g, one)
-
-    relay_back(1)
+                own_sum[b * BLK : (b + 1) * BLK, :] = sums[b]
+
+    relay_back(1, 0, z, True)
     far_forward(1)
     far_forward(0)
+    half = z // 2
+    relay_back(0, 0, half, False)
 
     arrived(xr.at[pl.ds(0, tp - 1)], x2r.at[0])
     arrived(dqr.at[pl.ds(0, r - 1)], dqr_sem.at[0])
@@ -460,24 +467,20 @@
         @pl.when(yy == y)
         def _():
             gw_ref[...] = total[yy * w : (yy + 1) * w]
-    for i in range(1, g):
+    for i in far_first(g):
         gw_copy(lax.rem(y + i, g), y).start()
 
-    relay_back(0)
+    relay_back(0, half, z, True)
     far_add(1)
     far_add(0)
 
-    arrived(gr.at[pl.ds(0, g - 1)], gr_sem.at[0])
-    for i in range(1, g):
-        gw_ref[...] += gr[lax.rem(y + i, g)].astype(F32)
-
     def settle(c):
         own_sum = gko if c == 0 else gvo
 
         def one(i):
             zz = z + 1 + i
 
-            @pl.when(~is_far(z, zz))
+            @pl.when(~is_far_back(z, zz))
             def _():
                 rel_copy(c, 0, zz).wait_recv()
                 own_sum[...] += rel_r[c, zz].astype(F32)
@@ -486,7 +489,11 @@
     settle(1)
     settle(0)
 
-    in_far = jnp.where(z == r - 1, 2, 0) + jnp.where(z == r - 2, 1, 0)
+    arrived(gr.at[pl.ds(0, g - 1)], gr_sem.at[0])
+    for i in range(1, g):
+        gw_ref[...] += gr[lax.rem(y + i, g)].astype(F32)
+
+    in_far = jnp.where(z == r - 1, 1, 0) + jnp.where(z == r - 2, 1, 0)
     counted(r - 1 - z - jnp.where(mine_far, 1, 0), r - 1, lambda i: left(kz.at[pl.ds(0, i)], zs_sem.at[0]))
     counted(g - 1 - y, g - 1, lambda i: left(kvs.at[z, pl.ds(0, i)], ys_sem.at[z]))
 
@@ -494,6 +501,9 @@
     def _():
         far_z_copy(z).wait_send()
         left(fs.at[pl.ds(0, g - 1)], fys.at[0])
+
+    @pl.when(mine_far_back)
+    def _():
         left(fb.at[0, pl.ds(0, g - 1)], frs.at[0])
         left(fb.at[1, pl.ds(0, g - 1)], frs.at[1])
 
@@ -502,14 +512,17 @@
         counted(y, g - 1, lambda i: left(back_s.at[c, z, pl.ds(0, i)], bs_sem.at[c, z]))
 
     def sent_row(zz):
-        @pl.when(is_far(zz, z))
+        @pl.when(~is_far(zz, z))
+        def _():
+            left(kvs.at[zz, pl.ds(0, g - 1)], ys_sem.at[zz])
+
+        @pl.when(is_far_back(zz, z))
         def _():
             far_back_copy(0, zz).wait_send()
             far_back_copy(1, zz).wait_send()
 
-        @pl.when(~is_far(zz, z))
-        def _():
-            left(kvs.at[zz, pl.ds(0, g - 1)], ys_sem.at[zz])
+        @pl.when(~is_far_back(zz, z))
+        def _():
             left(back_s.at[0, zz, pl.ds(0, g - 1)], bs_sem.at[0, zz])
             left(back_s.at[1, zz, pl.ds(0, g - 1)], bs_sem.at[1, zz])
     each(0, z, sent_row)
@@ -560,6 +573,7 @@
             pltpu.VMEM((r * g, 2, BLK, cols), BF16),
             pltpu.VMEM((r, g * BLK, wide), F32),
             pltpu.VMEM((r, g * BLK, wide), F32),
+            pltpu.VMEM((r, g * BLK, wide), BF16),
             pltpu.VMEM((2, r, g, BLK, cols), BF16),
             pltpu.VMEM((2, r, g, BLK, cols), BF16),
             pltpu.VMEM((2, r, tok, cols), BF16),

time: 65.9 us -> 62.4 us (0.947)
  the two profiles are of different devices: /device:TPU:12 before, /device:TPU:76 now
where the time goes in v4:
time: 62.4 us; the launch traced here: 62.1 us
  Pallas kernels  61.5 us (99%)
  between operations  0.64 us (1%)
    pallas_call x1, Pallas kernels, body(): pl.pallas_call(functools.partial(kernel, g, r, tp), out_shape=[jax.ShapeD...  60 us
    pallas_call x1, Pallas kernels, body(): pl.pallas_call(write_out, out_shape=[jax.ShapeDtypeStruct(a.shape, a.dtyp...  1.47 us

profile of v4, /device:TPU:76, one launch (start us, length us, event | category | flops | bytes accessed | tf_op | source)
XLA Modules:
  0.0 62.1 jit_solution(211091515437403674)
XLA Ops:
  0.6 60.0 %shard_map.102 = (bf16[128,128]{1,0:T(8,128)(2,1)}, bf16[128,128]{1,0:T(8,128)(2,1)}, bf16[128,128]{1,0:T(8,128)(2,1)}, f32[32,128]{1,0:T(8,128)}) custom-call(bf16[128,128]{1,0:T(8,128)(2,1)} %q_in.1, bf16[128,128]{1,0:T(8,128)(2,1)} %k_in.1, bf16[128,128]{1,0:T(8,128)(2,1)} %v_in.1, bf16[128,128]{1,0:T(8,128)(2,1)} %c_in.1, f32[2,128]{1,0:T(2,128)} %lse_in.1, ...), custom_call_target="tpu_custom_call" | custom-call | tf_op jit(solution)/shard_map/pallas_call | solution.py:555
  60.7 1.5 %shard_map.103 = (bf16[128,128]{1,0:T(8,128)(2,1)}, bf16[128,128]{1,0:T(8,128)(2,1)}, bf16[128,128]{1,0:T(8,128)(2,1)}, f32[32,128]{1,0:T(8,128)}) custom-call(bf16[128,128]{1,0:T(8,128)(2,1)} %get-tuple-element.8.refs_0_, bf16[128,128]{1,0:T(8,128)(2,1)} %get-tuple-element.9.refs_1_, bf16[128,128]{1,0:T(8,128)(2,1)} %get-tuple-element.10.refs_2_, ...), custom_call_target="tpu_custom_call" | custom-call | tf_op jit(solution)/shard_map/pallas_call | solution.py:610

commit v5 on v4

--- a/solution.py
+++ b/solution.py
@@ -232,7 +232,8 @@
             a, b = own_picked(r, yy)
             fs[yy, 0] = a
             fs[yy, 1] = b
-        each(1, g, lambda k: far_y_copy(lax.rem(y + k, g), y).start())
+        for k in far_first(g):
+            far_y_copy(lax.rem(y + k, g), y).start()
         ff[y] = fs[y]
 
     def own_rows(i):
@@ -242,18 +243,6 @@
         kvs[z, yy, 1] = b
         y_copy(z, yy, y).start()
     each(0, g - 1 - y, own_rows)
-
-    loads[3].wait()
-    width = x_ref.shape[1]
-    w = width // tp
-    eye = (iota((width, width), 0) == iota((width, width), 1)).astype(F32).astype(BF16)
-    flipped = dot(eye, x_ref[...], 1, 1).astype(BF16)
-    xs[...] = flipped.reshape(tp, w, tok)
-    each_x1(0, lambda s: x1_copy(s, z).start())
-
-    @pl.when(t == z)
-    def _():
-        xg[z] = xs[t]
 
     def clear(yy):
         kvt[z * g + yy] = jnp.zeros(kvt.shape[1:], BF16)
@@ -304,7 +293,8 @@
                               lambda b: kz[zz, 1, b * BLK : (b + 1) * BLK, :])
                 kvs[zz, yy, 0] = a
                 kvs[zz, yy, 1] = b
-            each(1, g, lambda k: y_copy(zz, lax.rem(y + k, g), y).start())
+            for k in far_first(g):
+                y_copy(zz, lax.rem(y + k, g), y).start()
             kvt[zz * g + y] = kvs[zz, y]
     once = jnp.minimum(z, 1)
     each(0, once, relay)
@@ -315,6 +305,18 @@
         far_z_copy(z).start()
     each(once, z, relay)
 
+    loads[3].wait()
+    width = x_ref.shape[1]
+    w = width // tp
+    eye = (iota((width, width), 0) == iota((width, width), 1)).astype(F32).astype(BF16)
+    flipped = dot(eye, x_ref[...], 1, 1).astype(BF16)
+    xs[...] = flipped.reshape(tp, w, tok)
+    each_x1(0, lambda s: x1_copy(s, z).start())
+
+    @pl.when(t == z)
+    def _():
+        xg[z] = xs[t]
+
     def send_back(c, zz):
         def one(k):
             yy = lax.rem(y + k, g)
@@ -329,7 +331,8 @@
 
         @pl.when(~is_far_back(zz, z))
         def _():
-            each(1, g, one)
+            for k in far_first(g):
+                one(k)
             back_r[c, zz, y] = back_s[c, zz, y]
 
     def pass_one(i, delta):
@@ -357,14 +360,7 @@
         back_s[1, zz] = dot(weights.astype(BF16), cs[...], 1, 0).astype(BF16).reshape(g, BLK, cols)
         send_back(1, zz)
         return delta + jnp.sum(weights * vd, axis=0, keepdims=True)
-    middle = (z + 2) // 2
-    delta = lax.fori_loop(0, middle, pass_one, first)
-
-    counted(tp - jnp.where(t == z, 1, 0), tp, lambda i: arrived(xg.at[pl.ds(0, i)], x1r.at[0]))
-    for i in range(1, tp):
-        x2_copy(lax.rem(t + i, tp), t).start()
-    xr[t] = xg[...]
-    delta = lax.fori_loop(middle, z + 1, pass_one, delta)
+    delta = lax.fori_loop(0, z + 1, pass_one, first)
 
     dso = (own * (vdo - delta)).astype(BF16)
     dqa[...] = dot(dso, k_ref[...], 0, 0)
@@ -396,6 +392,11 @@
         def _():
             key_grads(zz)
     each(0, z + 1, other_key_grads)
+
+    counted(tp - jnp.where(t == z, 1, 0), tp, lambda i: arrived(xg.at[pl.ds(0, i)], x1r.at[0]))
+    for i in range(1, tp):
+        x2_copy(lax.rem(t + i, tp), t).start()
+    xr[t] = xg[...]
     gko[...] = dot(dso, qs[...], 1, 0) * scale
 
     def relay_back(c, low_z, high_z, with_own):
@@ -431,7 +432,7 @@
         @pl.when(mine_far_back)
         def _():
             far_back_copy(c, 0).wait_recv()
-            for i in range(1, g):
+            for i in far_first(g):
                 far_ret_copy(c, lax.rem(y + i, g), y).start()
 
     def far_add(c):

time: 62.4 us -> 62.2 us (level)
  the two profiles are of different devices: /device:TPU:76 before, /device:TPU:78 now
where the time goes in v5:
time: 62.2 us; the launch traced here: 61.9 us
  Pallas kernels  61.3 us (99%)
  between operations  0.64 us (1%)
    pallas_call x1, Pallas kernels, body(): pl.pallas_call(functools.partial(kernel, g, r, tp), out_shape=[jax.ShapeD...  59.8 us
    pallas_call x1, Pallas kernels, body(): pl.pallas_call(write_out, out_shape=[jax.ShapeDtypeStruct(a.shape, a.dtyp...  1.47 us

profile of v5, /device:TPU:78, one launch (start us, length us, event | category | flops | bytes accessed | tf_op | source)
XLA Modules:
  0.0 61.9 jit_solution(12182422925694770539)
XLA Ops:
  0.6 59.8 %shard_map.102 = (bf16[128,128]{1,0:T(8,128)(2,1)}, bf16[128,128]{1,0:T(8,128)(2,1)}, bf16[128,128]{1,0:T(8,128)(2,1)}, f32[32,128]{1,0:T(8,128)}) custom-call(bf16[128,128]{1,0:T(8,128)(2,1)} %q_in.1, bf16[128,128]{1,0:T(8,128)(2,1)} %k_in.1, bf16[128,128]{1,0:T(8,128)(2,1)} %v_in.1, bf16[128,128]{1,0:T(8,128)(2,1)} %c_in.1, f32[2,128]{1,0:T(2,128)} %lse_in.1, ...), custom_call_target="tpu_custom_call" | custom-call | tf_op jit(solution)/shard_map/pallas_call | solution.py:556
  60.5 1.5 %shard_map.103 = (bf16[128,128]{1,0:T(8,128)(2,1)}, bf16[128,128]{1,0:T(8,128)(2,1)}, bf16[128,128]{1,0:T(8,128)(2,1)}, f32[32,128]{1,0:T(8,128)}) custom-call(bf16[128,128]{1,0:T(8,128)(2,1)} %get-tuple-element.8.refs_0_, bf16[128,128]{1,0:T(8,128)(2,1)} %get-tuple-element.9.refs_1_, bf16[128,128]{1,0:T(8,128)(2,1)} %get-tuple-element.10.refs_2_, ...), custom_call_target="tpu_custom_call" | custom-call | tf_op jit(solution)/shard_map/pallas_call | solution.py:611

commit v6 on v5

--- a/solution.py
+++ b/solution.py
@@ -106,7 +106,7 @@
         return remote(kv_ref, kz.at[slot], zs_sem.at[0], zr_sem.at[slot], zz * g + y, t)
 
     def y_copy(zz, yy, slot):
-        return remote(kvs.at[zz, yy], kvt.at[zz * g + slot], ys_sem.at[zz], yr_sem.at[zz], z * g + yy, t)
+        return remote(kvs.at[zz, yy], kvt.at[zz * g + slot], ys_sem.at[0], yr_sem.at[zz], z * g + yy, t)
 
     def far_y_copy(yy, slot):
         return remote(fs.at[yy], ff.at[slot], fys.at[0], fyr.at[0], z * g + yy, t)
@@ -121,7 +121,7 @@
         return remote(fb.at[c, yy], fr.at[c, slot], frs.at[c], frr.at[c], z * g + yy, t)
 
     def back_copy(c, zz, yy, slot):
-        return remote(back_s.at[c, zz, yy], back_r.at[c, zz, slot], bs_sem.at[c, zz], br_sem.at[c, zz], z * g + yy, t)
+        return remote(back_s.at[c, zz, yy], back_r.at[c, zz, slot], bs_sem.at[c], br_sem.at[c, zz], z * g + yy, t)
 
     def rel_copy(c, zz, slot):
         return remote(rel_s.at[c, zz], rel_r.at[c, slot], rs_sem.at[c], rr_sem.at[c, slot], zz * g + y, t)
@@ -362,6 +362,11 @@
         return delta + jnp.sum(weights * vd, axis=0, keepdims=True)
     delta = lax.fori_loop(0, z + 1, pass_one, first)
 
+    counted(tp - jnp.where(t == z, 1, 0), tp, lambda i: arrived(xg.at[pl.ds(0, i)], x1r.at[0]))
+    for i in range(1, tp):
+        x2_copy(lax.rem(t + i, tp), t).start()
+    xr[t] = xg[...]
+
     dso = (own * (vdo - delta)).astype(BF16)
     dqa[...] = dot(dso, k_ref[...], 0, 0)
 
@@ -392,11 +397,6 @@
         def _():
             key_grads(zz)
     each(0, z + 1, other_key_grads)
-
-    counted(tp - jnp.where(t == z, 1, 0), tp, lambda i: arrived(xg.at[pl.ds(0, i)], x1r.at[0]))
-    for i in range(1, tp):
-        x2_copy(lax.rem(t + i, tp), t).start()
-    xr[t] = xg[...]
     gko[...] = dot(dso, qs[...], 1, 0) * scale
 
     def relay_back(c, low_z, high_z, with_own):
@@ -496,7 +496,7 @@
 
     in_far = jnp.where(z == r - 1, 1, 0) + jnp.where(z == r - 2, 1, 0)
     counted(r - 1 - z - jnp.where(mine_far, 1, 0), r - 1, lambda i: left(kz.at[pl.ds(0, i)], zs_sem.at[0]))
-    counted(g - 1 - y, g - 1, lambda i: left(kvs.at[z, pl.ds(0, i)], ys_sem.at[z]))
+    counted(g - 1 - y, g - 1, lambda i: left(kvs.at[z, pl.ds(0, i)], ys_sem.at[0]))
 
     @pl.when(mine_far)
     def _():
@@ -510,12 +510,12 @@
 
     for c in range(2):
         counted(z - in_far, r - 1, lambda i: left(rel_s.at[c, pl.ds(0, i)], rs_sem.at[c]))
-        counted(y, g - 1, lambda i: left(back_s.at[c, z, pl.ds(0, i)], bs_sem.at[c, z]))
+        counted(y, g - 1, lambda i: left(back_s.at[c, z, pl.ds(0, i)], bs_sem.at[c]))
 
     def sent_row(zz):
         @pl.when(~is_far(zz, z))
         def _():
-            left(kvs.at[zz, pl.ds(0, g - 1)], ys_sem.at[zz])
+            left(kvs.at[zz, pl.ds(0, g - 1)], ys_sem.at[0])
 
         @pl.when(is_far_back(zz, z))
         def _():
@@ -524,8 +524,8 @@
 
         @pl.when(~is_far_back(zz, z))
         def _():
-            left(back_s.at[0, zz, pl.ds(0, g - 1)], bs_sem.at[0, zz])
-            left(back_s.at[1, zz, pl.ds(0, g - 1)], bs_sem.at[1, zz])
+            left(back_s.at[0, zz, pl.ds(0, g - 1)], bs_sem.at[0])
+            left(back_s.at[1, zz, pl.ds(0, g - 1)], bs_sem.at[1])
     each(0, z, sent_row)
     counted(tp - jnp.where(t == z, 1, 0), tp, lambda i: left(xs.at[pl.ds(0, i)], x1s.at[0]))
     left(xr.at[pl.ds(0, tp - 1)], x2s.at[0])
@@ -593,8 +593,8 @@
             pltpu.VMEM((2, g, BLK, cols), BF16),
             pltpu.VMEM((2, g, BLK, cols), BF16),
             sem((1,)), sem((r,)),
-            sem((r,)), sem((r,)),
-            sem((2, r)), sem((2, r)),
+            sem((1,)), sem((r,)),
+            sem((2,)), sem((2, r)),
             sem((2,)), sem((2, r)),
             sem((1,)), sem((1,)),
             sem((1,)), sem((1,)),

time: 62.2 us -> 62.1 us (level)
  the two profiles are of different devices: /device:TPU:78 before, /device:TPU:1 now
where the time goes in v6:
time: 62.1 us; the launch traced here: 61.9 us
  Pallas kernels  61.3 us (99%)
  between operations  0.64 us (1%)
    pallas_call x1, Pallas kernels, body(): pl.pallas_call(functools.partial(kernel, g, r, tp), out_shape=[jax.ShapeD...  59.8 us
    pallas_call x1, Pallas kernels, body(): pl.pallas_call(write_out, out_shape=[jax.ShapeDtypeStruct(a.shape, a.dtyp...  1.47 us

profile of v6, /device:TPU:1, one launch (start us, length us, event | category | flops | bytes accessed | tf_op | source)
XLA Modules:
  0.0 61.9 jit_solution(17860765116284645409)
XLA Ops:
  0.6 59.8 %shard_map.102 = (bf16[128,128]{1,0:T(8,128)(2,1)}, bf16[128,128]{1,0:T(8,128)(2,1)}, bf16[128,128]{1,0:T(8,128)(2,1)}, f32[32,128]{1,0:T(8,128)}) custom-call(bf16[128,128]{1,0:T(8,128)(2,1)} %q_in.1, bf16[128,128]{1,0:T(8,128)(2,1)} %k_in.1, bf16[128,128]{1,0:T(8,128)(2,1)} %v_in.1, bf16[128,128]{1,0:T(8,128)(2,1)} %c_in.1, f32[2,128]{1,0:T(2,128)} %lse_in.1, ...), custom_call_target="tpu_custom_call" | custom-call | tf_op jit(solution)/shard_map/pallas_call | solution.py:556
  60.5 1.5 %shard_map.103 = (bf16[128,128]{1,0:T(8,128)(2,1)}, bf16[128,128]{1,0:T(8,128)(2,1)}, bf16[128,128]{1,0:T(8,128)(2,1)}, f32[32,128]{1,0:T(8,128)}) custom-call(bf16[128,128]{1,0:T(8,128)(2,1)} %get-tuple-element.8.refs_0_, bf16[128,128]{1,0:T(8,128)(2,1)} %get-tuple-element.9.refs_1_, bf16[128,128]{1,0:T(8,128)(2,1)} %get-tuple-element.10.refs_2_, ...), custom_call_target="tpu_custom_call" | custom-call | tf_op jit(solution)/shard_map/pallas_call | solution.py:611
